TPU v7x, 128 devices: a whole 4x4x4 slice. The times are simulated.
128 devices in a mesh: sp: 16 (over z, x), tp: 8 (over y, core).
Axes of the slice: x: 4, y: 4, z: 4, core: 2. Of those that a mesh axis runs over, the one named last changes fastest.
Arguments:
- queries: bfloat16 [16384, 1024], P('sp', 'tp'), may hold values from -6 to 6, as said below
- key_rows: bfloat16 [16384, 1024], P('sp', 'tp'), may hold values from -6 to 6, as said below
- value_rows: bfloat16 [16384, 1024], P('sp', 'tp'), may hold values from -6 to 6
- lambdas: float32 [8], P('tp'), may hold values from 0.3 to 0.8
- head_gain: float32 [128], replicated, may hold values from 0.1 to 1.9
- out_weight: bfloat16 [1024, 2048], replicated, may hold values from -0.1875 to 0.1875
- stream: bfloat16 [16384, 2048], P(('sp', 'tp')), may hold values from -6 to 6
- ffn_gain: float32 [2048], replicated, may hold values from 0.1 to 1.9
- routes: int32 [16384, 2], P(('sp', 'tp')), may hold values from 0 to 15, all different within a row; in each aligned block of 128 rows (0 to 127, 128 to 255, ...) at most 20 rows name the same one
- route_weight: float32 [16384, 2], P(('sp', 'tp')), may hold values from 0.1 to 1
- gate_weight: bfloat16 [16, 2048, 5120], P('sp', None, 'tp'), may hold values from -0.125 to 0.125
- up_weight: bfloat16 [16, 2048, 5120], P('sp', None, 'tp'), may hold values from -0.125 to 0.125
- down_weight: bfloat16 [16, 5120, 2048], P('sp', 'tp'), may hold values from -0.078125 to 0.078125
Outputs:
- layer_out: bfloat16 [16384, 2048], P(('sp', 'tp'))
Inputs may be any that keep to these rules, and one draw needn't show every extreme that they name: Custom draw; the queries of a position meet only keys of the same or earlier positions. `key_rows`: custom draw. `routes`: each row names 2 different experts. In the 128 rows of one device no expert is named by more than 20 rows, and every draw reaches 20 on some device.
All inputs are finite; a program needn't handle non-finite values.
Results may differ from a plain program's by a relative error of at most 0.01.
Values may be sent and summed in bfloat16 or wider, within the bound.
A program may use at most 128 MiB of HBM per device.

v0:
```python
import math

import jax
import jax.numpy as jnp
from jax import lax
from jax.sharding import PartitionSpec as P

DH = 64


def side_by_side(arrays, axis, dim, along):
    both = jnp.concatenate(arrays, axis=along)
    filled, at, gathered = (lax.all_gather(both, axis, axis=dim, tiled=True), 0, [])
    for a in arrays:
        gathered.append(lax.slice_in_dim(filled, at, at + a.shape[along], axis=along))
        at += a.shape[along]
    return tuple(gathered)


def expert_rows(rows_in, gate_local, up_local, down_local):
    flat = rows_in.reshape(-1, rows_in.shape[-1])
    gate = jnp.dot(flat, gate_local, preferred_element_type=jnp.float32)
    upper = jnp.dot(flat, up_local, preferred_element_type=jnp.float32)
    act = (jax.nn.silu(gate) * upper).astype(jnp.bfloat16)
    result = jnp.dot(act, down_local, preferred_element_type=jnp.float32)
    return result.reshape(rows_in.shape)


def local(
    queries,
    key_rows,
    value_rows,
    lambdas,
    head_gain,
    out_weight,
    stream,
    ffn_gain,
    routes,
    route_weight,
    gate_weight,
    up_weight,
    down_weight,
):
    length = queries.shape[0]
    head_count = queries.shape[1] // (2 * DH)
    query_heads = queries.reshape(length, head_count, 2, DH)
    offset = lax.axis_index("sp") * length
    query_pos = offset + jnp.arange(length, dtype=jnp.int32)
    last_pos = offset + length - 1
    scale = DH ** (-0.5)
    initial = (
        jnp.full((head_count, 2, length), -1e30, jnp.float32),
        jnp.zeros((head_count, 2, length), jnp.float32),
        jnp.zeros((head_count, 2, length, 2 * DH), jnp.float32),
    )
    key_piece, value_piece = side_by_side((key_rows, value_rows), "sp", 0, 1)
    count = key_piece.shape[0]
    block = math.gcd(count, 512)

    def advance(number, state):
        begin = number * block
        key_block = lax.dynamic_slice_in_dim(key_piece, begin, block, 0).reshape(
            block, head_count, 2, DH
        )
        value_block = lax.dynamic_slice_in_dim(value_piece, begin, block, 0).reshape(
            block, head_count, 2 * DH
        )
        key_pos = begin + jnp.arange(block, dtype=jnp.int32)

        def compute(inner):
            maxima, totals, accum = inner
            scores = (
                jnp.einsum(
                    "qhmd,khmd->hmqk", query_heads, key_block, preferred_element_type=jnp.float32
                )
                * scale
            )
            mask = key_pos[None, :] <= query_pos[:, None]
            scores = jnp.where(mask, scores, -jnp.inf)
            fresh = jnp.maximum(maxima, jnp.max(scores, axis=-1))
            expo = jnp.exp(scores - fresh[..., None])
            factor = jnp.exp(maxima - fresh)
            totals = totals * factor + jnp.sum(expo, axis=-1)
            accum = accum * factor[..., None] + jnp.einsum(
                "hmqk,khe->hmqe",
                expo.astype(jnp.bfloat16),
                value_block,
                preferred_element_type=jnp.float32,
            )
            return (fresh, totals, accum)

        return lax.cond(begin <= last_pos, compute, lambda inner: inner, state)

    maxima, totals, accum = lax.fori_loop(0, count // block, advance, initial)
    mixed = accum / totals[..., None]
    contrast = mixed[:, 0] - lambdas[:, None, None] * mixed[:, 1]
    contrast = (
        contrast
        * lax.rsqrt(jnp.mean(contrast * contrast, axis=-1, keepdims=True) + 1e-05)
        * head_gain
    )
    heads_out = (
        jnp.transpose(contrast, (1, 0, 2)).reshape(length, head_count * 2 * DH).astype(jnp.bfloat16)
    )
    heads_local = lax.all_to_all(heads_out, "tp", split_axis=0, concat_axis=1, tiled=True)
    attended = stream.astype(jnp.float32) + jnp.dot(
        heads_local, out_weight, preferred_element_type=jnp.float32
    )
    normed = (
        attended
        * lax.rsqrt(jnp.mean(attended * attended, axis=-1, keepdims=True) + 1e-06)
        * ffn_gain
    ).astype(jnp.bfloat16)
    rows_local = normed.shape[0]
    width = normed.shape[1]
    top_count = routes.shape[1]
    sp_size = lax.axis_size("sp")
    experts = sp_size * gate_weight.shape[0]
    slots = max(2, (rows_local * top_count * 5 + 4 * experts - 1) // (4 * experts))
    flat_routes = routes.reshape(-1)
    onehot = (flat_routes[:, None] == jnp.arange(experts, dtype=jnp.int32)[None, :]).astype(
        jnp.int32
    )
    before = jnp.cumsum(onehot, axis=0) - onehot
    slot = jnp.sum(before * onehot, axis=1)
    target = flat_routes * slots + slot
    placed = (target[:, None] == jnp.arange(experts * slots, dtype=jnp.int32)[None, :]).astype(
        jnp.float32
    )
    placed = placed.reshape(rows_local, top_count, experts * slots)
    dispatch = jnp.transpose(jnp.sum(placed, axis=1)).astype(jnp.bfloat16)
    combine = jnp.einsum("tk,tks->ts", route_weight, placed)
    outgoing = (
        jnp.dot(dispatch, normed, preferred_element_type=jnp.float32)
        .astype(jnp.bfloat16)
        .reshape(experts, slots, width)
    )
    gate_local = gate_weight[0]
    up_local = up_weight[0]
    down_local = down_weight[0]
    arrived = lax.all_to_all(outgoing, "sp", split_axis=0, concat_axis=0, tiled=True)
    partial_value = expert_rows(
        lax.all_gather(arrived[:, None], "tp", axis=1, tiled=True), gate_local, up_local, down_local
    )
    summed = lax.psum_scatter(
        partial_value.astype(jnp.bfloat16), "tp", scatter_dimension=1, tiled=True
    )
    returned = lax.all_to_all(summed, "sp", split_axis=0, concat_axis=0, tiled=True).reshape(
        experts * slots, width
    )
    routed = jnp.dot(combine, returned.astype(jnp.float32))
    return (attended + routed).astype(jnp.bfloat16)


def solution(mesh):
    placed = (
        P("sp", "tp"),
        P("sp", "tp"),
        P("sp", "tp"),
        P("tp"),
        P(),
        P(),
        P(("sp", "tp"), None),
        P(),
        P(("sp", "tp"), None),
        P(("sp", "tp"), None),
        P("sp", None, "tp"),
        P("sp", None, "tp"),
        P("sp", "tp", None),
    )
    return jax.shard_map(
        local, mesh=mesh, in_specs=placed, out_specs=P(("sp", "tp"), None), check_vma=False
    )
```

profile of v0, /device:TPU:1, one launch (start us, length us, event | category | flops | bytes accessed | tf_op | source)
XLA Modules:
  0.0 603.9 jit_solution(11017342687480843919)
XLA Ops:
  6.5 2.0 pad_maximum_fusion
  8.6 0.8 copy.91
  10.3 0.6 reduce-window.6
  10.9 0.2 slice_reduce_fusion
  11.2 0.1 reduce_sum.51
  11.5 1.1 copy.88
  12.6 70.9 %all-gather.4.cloned.1.call-done = bf16[16384,256]{1,0:T(8,128)(2,1)} async-done(((bf16[1024,256]{1,0:T(8,128)(2,1)}), bf16[16384,256]{1,0:T(8,128)(2,1)}) %all-gather.4.cloned.1.call-update) | async-done | bytes 8388624 | tf_op jit(solution)/shard_map/all_gather | solution.py:13
  83.5 5.7 fusion.36
  89.2 6.4 %copy.89 = bf16[16384,128]{0,1:T(8,128)(2,1)} copy(bf16[16384,128]{1,0:T(8,128)(2,1)} %get-tuple-element.414) | data formatting | bytes 8388608
  95.6 1.0 broadcast_in_dim.22
  96.6 16.0 %while.18 = (s32[]{:T(128)}, f32[1,2,1024]{2,1,0:T(2,128)S(1)}, f32[1,2,1024]{2,1,0:T(2,128)S(1)}, f32[1,2,1024,128]{3,2,1,0:T(8,128)}, s32[]{:T(128)}, /*index=...) while((s32[]{:T(128)}, f32[1,2,1024]{2,1,0:T(2,128)S(1)}, ...), condition=%wide.region_5.6_spmd.clone, body=%wide.region_0.5_spmd.clone.sunk | while | flops 415243776 | bytes 17719616 | solution.py:94
  96.7 7.0 %conditional.3 = ((f32[1,2,1024]{2,1,0:T(2,128)S(1)}, f32[1,2,1024]{2,1,0:T(2,128)S(1)}, f32[1,2,1024,128]{3,2,1,0:T(8,128)})) conditional(s32[]{:T(128)} %convert_element_type.84, (f32[1,2,1024]{2,1,0:T(2,128)S(1)}, f32[1,2,1024]{2,1,0:T(2,128)S(1)}, f32[1,2,1024,128]{3,2,1,0:T(8,128)}) %tuple.65, (s32[]{:T(128)}, s32[512]{0:T(512)S(1)}, s32[]{:T(128)}, ...), branch_computations={%region_1.0_spmd, %region_2.4_spmd} | conditional | flops 415243776 | bytes 17713234 | solution.py:92
  96.7 0.9 constant_dynamic-slice_fusion
  97.6 0.4 broadcast_compare_fusion
  98.0 1.0 fusion.4
  99.0 3.6 fusion.11
  102.6 1.0 fusion.3
  103.7 7.0 %conditional.3 = ((f32[1,2,1024]{2,1,0:T(2,128)S(1)}, f32[1,2,1024]{2,1,0:T(2,128)S(1)}, f32[1,2,1024,128]{3,2,1,0:T(8,128)})) conditional(s32[]{:T(128)} %convert_element_type.84, (f32[1,2,1024]{2,1,0:T(2,128)S(1)}, f32[1,2,1024]{2,1,0:T(2,128)S(1)}, f32[1,2,1024,128]{3,2,1,0:T(8,128)}) %tuple.65, (s32[]{:T(128)}, s32[512]{0:T(512)S(1)}, s32[]{:T(128)}, ...), branch_computations={%region_1.0_spmd, %region_2.4_spmd} | conditional | flops 415243776 | bytes 17713234 | solution.py:92
  103.7 0.9 constant_dynamic-slice_fusion
  104.7 0.4 broadcast_compare_fusion
  105.0 1.0 fusion.4
  106.1 3.6 fusion.11
  109.7 1.0 fusion.3
  112.7 1.6 broadcast_divide_fusion
  114.3 0.2 multiply_reduce_fusion.1
  114.6 0.9 multiply_convert_fusion.3
  115.5 5.1 all-to-all-start
  120.7 6.4 %all-to-all-done = bf16[8,128,128]{2,1,0:T(8,128)(2,1)S(1)} async-done(((bf16[8,128,128]{2,1,0:T(8,128)(2,1)}), bf16[8,128,128]{2,1,0:T(8,128)(2,1)S(1)}, u32[]{:S(2)}, u32[]{:S(2)}) %all-to-all-start) | async-done | bytes 262176 | tf_op jit(solution)/shard_map/all_to_all | solution.py:105
  127.1 0.2 copy.90
  127.3 3.1 multiply_reduce_fusion
  130.4 1.0 copy-done.2
  131.4 1.6 convolution_convert_fusion.1
  133.0 3.2 reshape.225
  136.2 235.9 %all_to_all.26 = bf16[16,20,2048]{2,1,0:T(8,128)(2,1)S(1)} all-to-all(bf16[16,20,2048]{2,1,0:T(8,128)(2,1)} %reshape.225), channel_id=1, replica_groups=mesh['sp'=16,'tp'=8] {'sp'}, dimensions={0} | all-to-all | bytes 2621440 | tf_op jit(solution)/shard_map/all_to_all | solution.py:141
  372.1 1.8 copy.95
  373.9 0.2 reduce-scatter.2.cloned.1.call-start
  374.2 55.9 %all-gather.6.cloned.1.call-done = bf16[16,160,2048]{2,0,1:T(8,128)(2,1)} async-done(((bf16[16,20,2048]{2,0,1:T(8,128)(2,1)}), bf16[16,160,2048]{2,0,1:T(8,128)(2,1)}) %all-gather.6.cloned.1.call-update) | async-done | bytes 10485776 | tf_op jit(solution)/shard_map/all_gather | solution.py:143
  430.1 13.6 %copy.96 = bf16[16,160,2048]{2,1,0:T(8,128)(2,1)} copy(bf16[16,160,2048]{2,0,1:T(8,128)(2,1)} %all-gather.6.cloned.1.call-done) | data formatting | bytes 20971520 | tf_op jit(solution)/shard_map/all_gather | solution.py:143
  443.7 12.4 %fusion.24 = f32[2560,640]{1,0:T(8,128)S(1)} fusion(bf16[2560,2048]{1,0:T(8,128)(2,1)} %bitcast.85, bf16[1,2048,640]{2,1,0:T(8,128)(2,1)} %param.27), kind=kOutput, calls=%fused_computation.30 | convolution fusion | flops 6710886400 | bytes 19660800 | tf_op jit(solution)/shard_map/dot_general | solution.py:22
  456.2 10.4 %multiply_convert_fusion = bf16[2560,640]{1,0:T(8,128)(2,1)} fusion(f32[2560,640]{1,0:T(8,128)S(1)} %fusion.24, bf16[2560,2048]{1,0:T(8,128)(2,1)S(1)} %bitcast.86, bf16[1,2048,640]{2,1,0:T(8,128)(2,1)S(1)} %copy-done.7), kind=kOutput, calls=%fused_computation.26 | convolution fusion | flops 6720716800 | bytes 22937600 | tf_op jit(solution)/shard_map/dot_general | solution.py:23
  466.6 6.1 %dot_general.36 = bf16[16,8,20,640]{3,2,1,0:T(8,128)(2,1)} reshape(bf16[2560,640]{1,0:T(8,128)(2,1)} %multiply_convert_fusion) | data formatting | bytes 6553600 | tf_op jit(solution)/shard_map/dot_general | solution.py:25
  472.7 12.7 %convolution_convert_fusion = bf16[16,8,20,2048]{3,2,1,0:T(8,128)(2,1)S(1)} fusion(bf16[16,8,20,640]{3,2,1,0:T(8,128)(2,1)} %dot_general.36, bf16[1,640,2048]{2,1,0:T(8,128)(2,1)S(1)} %copy-done), kind=kOutput, calls=%fused_computation.25 | convolution fusion | flops 6716129280 | bytes 16384000 | tf_op jit(solution)/shard_map/dot_general | solution.py:25
  485.4 13.9 %copy.97 = bf16[16,8,20,2048]{3,0,2,1:T(8,128)(2,1)} copy(bf16[16,8,20,2048]{3,2,1,0:T(8,128)(2,1)S(1)} %convolution_convert_fusion) | data formatting | bytes 20971520 | tf_op jit(solution)/shard_map/convert_element_type | solution.py:146
  499.3 61.9 %reduce-scatter.2.cloned.1.call-done = bf16[16,1,20,2048]{3,0,2,1:T(8,128)(2,1)} async-done(((bf16[16,8,20,2048]{3,0,2,1:T(8,128)(2,1)}), bf16[16,1,20,2048]{3,0,2,1:T(8,128)(2,1)}) %reduce-scatter.2.cloned.1.call-update) | async-done | bytes 1310736 | tf_op jit(solution)/shard_map/reduce_scatter | solution.py:145
  561.2 2.0 copy.98
  563.2 28.0 %all_to_all.27 = bf16[16,1,20,2048]{3,2,1,0:T(8,128)(2,1)} all-to-all(bf16[16,1,20,2048]{3,2,1,0:T(8,128)(2,1)S(1)} %copy.98), channel_id=1, replica_groups=mesh['sp'=16,'tp'=8] {'sp'}, dimensions={0} | all-to-all | bytes 2621440 | tf_op jit(solution)/shard_map/all_to_all | solution.py:148
  591.2 3.3 reshape.227
  594.5 2.9 fusion.26
  (137 shorter events, 1.4 us)
Async XLA Ops:
  6.5 466.1 %copy-start = (bf16[1,640,2048]{2,1,0:T(8,128)(2,1)S(1)}, bf16[1,640,2048]{2,1,0:T(8,128)(2,1)}, u32[]{:S(2)}) copy-start(bf16[1,640,2048]{2,1,0:T(8,128)(2,1)} %param.29) | copy-start | bytes 7864324
  6.5 76.9 %all-gather.4.cloned.1.call-start = ((), (), s32[]{:S(2)}) async-start(), calls=%async_computation.4 | async-start | bytes 8912896 | tf_op jit(solution)/shard_map/all_gather | solution.py:13
  96.6 17.9 %copy-start.6 = (f32[128]{0:T(128)S(1)}, f32[128]{0:T(128)}, u32[]{:S(2)}) copy-start(f32[128]{0:T(128)} %param.21) | copy-start | bytes 1540
  112.7 7.9 %copy-start.4 = (s32[128,2]{0,1:T(2,128)S(1)}, s32[128,2]{0,1:T(2,128)}, u32[]{:S(2)}) copy-start(s32[128,2]{0,1:T(2,128)} %param.25) | copy-start | bytes 3076
  112.7 7.9 %copy-start.5 = (f32[128,2]{0,1:T(2,128)S(1)}, f32[128,2]{0,1:T(2,128)}, u32[]{:S(2)}) copy-start(f32[128,2]{0,1:T(2,128)} %param.26) | copy-start | bytes 3076
  114.5 16.8 %copy-start.3 = (f32[2048]{0:T(1024)S(1)}, f32[2048]{0:T(1024)}, u32[]{:S(2)}) copy-start(f32[2048]{0:T(1024)} %param.24) | copy-start | bytes 24580
  115.5 11.6 %all-to-all-start = ((bf16[8,128,128]{2,1,0:T(8,128)(2,1)}), bf16[8,128,128]{2,1,0:T(8,128)(2,1)S(1)}, u32[]{:S(2)}, u32[]{:S(2)}) async-start(bf16[8,128,128]{2,1,0:T(8,128)(2,1)} %multiply_convert_fusion.3), calls=%async_computation | async-start | bytes 524288 | tf_op jit(solution)/shard_map/all_to_all | solution.py:105
  120.6 309.5 %all-gather.6.cloned.1.call-start = ((), (), s32[]{:S(2)}) async-start(), calls=%async_computation.6 | async-start | bytes 11796480 | tf_op jit(solution)/shard_map/all_gather | solution.py:143
  130.4 1.0 copy-start.2
  373.9 187.2 %reduce-scatter.2.cloned.1.call-start = ((), (), s32[]{:S(2)}) async-start(), calls=%async_computation.5 | async-start | bytes 11796480 | tf_op jit(solution)/shard_map/reduce_scatter | solution.py:145
  443.7 12.5 %copy-start.1 = (bf16[16,160,2048]{2,1,0:T(8,128)(2,1)S(1)}, bf16[16,160,2048]{2,1,0:T(8,128)(2,1)}, u32[]{:S(2)}) copy-start(bf16[16,160,2048]{2,1,0:T(8,128)(2,1)} %copy.96) | copy-start | bytes 31457284
  443.7 12.5 %copy-start.7 = (bf16[1,2048,640]{2,1,0:T(8,128)(2,1)S(1)}, bf16[1,2048,640]{2,1,0:T(8,128)(2,1)}, u32[]{:S(2)}) copy-start(bf16[1,2048,640]{2,1,0:T(8,128)(2,1)} %param.28) | copy-start | bytes 7864324
Sparse Core Ops, SparseCore 0:
  9.5 73.9 all-gather.3
  374.1 55.9 all-gather.5
  499.4 61.7 reduce-scatter.1
where the time goes:
time: 608 us; the launch traced here: 604 us
  blocking collectives  264 us (43%)
  waiting for transfers between devices  195 us (32%)
  local copies, waits for them, and re-layouts  62.8 us (10%)
  matrix products  52.5 us (9%)
  between operations  14 us (2%)
  other arithmetic  8.29 us (1%)
    all_to_all x1, blocking collectives, local(): lax.all_to_all(outgoing, 'sp', split_axis=0, concat_axis=0, tiled=True)  236 us
    all_gather x1, waiting for transfers between devices, side_by_side(): lax.all_gather(both, axis, axis=dim, tiled=True)  70.9 us
    reduce_scatter x1, waiting for transfers between devices, local(): lax.psum_scatter(partial_value.astype(jnp.bfloat16), 'tp', scatter_dimens...  61.9 us
    all_gather x1, waiting for transfers between devices, local(): lax.all_gather(arrived[:, None], 'tp', axis=1, tiled=True)  55.9 us
    all_to_all x1, blocking collectives, local(): lax.all_to_all(summed, 'sp', split_axis=0, concat_axis=0, tiled=True)  28 us
    convert_element_type x1, local copies, waits for them, and re-layouts, local(): partial_value.astype(jnp.bfloat16)  13.9 us
    all_gather x1, local copies, waits for them, and re-layouts, local(): lax.all_gather(arrived[:, None], 'tp', axis=1, tiled=True)  13.6 us
    dot_general x1, matrix products, expert_rows(): result = jnp.dot(act, down_local, preferred_element_type=jnp.float32)  12.7 us
  transfers between devices with their start and end apart: 4, of which 4 were waited for; matrix products, arithmetic and copies ran while one was open for 1% of the time, Pallas kernels for 0%

commit v1 on v0

v1 whole, which is shorter than its diff:
```python
import jax
import jax.numpy as jnp
from jax import lax
from jax.experimental import pallas as pl
from jax.experimental.pallas import tpu as pltpu
from jax.sharding import PartitionSpec as P

DH = 64


LOG2E = 1.4426950408889634
MESH = pl.DeviceIdType.MESH
NZ = 4
NX = 4
BLK = 1024
HALF = 512
ORDER = (
    (0, 0), (0, -1), (0, 1), (-1, 0), (1, 0), (-1, -1), (-1, 1), (1, -1), (1, 1),
    (0, 2), (2, 0), (-1, 2), (2, -1), (1, 2), (2, 1), (2, 2),
)
EVENTS = {
    1: [((0, -1), (-1, 0)), ((0, 1), (1, 0)), ((-1, 0), (0, -1)), ((1, 0), (0, 1))],
    3: [((0, 2), (2, 0))],
    5: [((-1, -1), (-1, -1)), ((1, -1), (-1, 1))],
    6: [((-1, 1), (1, -1)), ((1, 1), (1, 1))],
    9: [((2, 0), (0, 2))],
    10: [((-1, 2), (2, -1)), ((1, 2), (2, 1))],
    11: [((2, -1), (-1, 2))],
    13: [((2, 1), (1, 2))],
    15: [((2, 2), (2, 2))],
}


def attention_kernel(
    lam_ref, gain_ref, q_hbm, k_hbm, v_hbm, out_ref,
    kv, qin, qs, mx, acc, obuf,
    load_sem, qsend, qrecv, send_sem, recv_sem, osend, orecv,
):
    s = lax.axis_index("sp")
    t = lax.axis_index("tp")
    z, x = s // NX, s % NX
    mirror = NZ * NX - 1 - s

    def at(dz, dx):
        return ((z + dz + NZ) % NZ) * NX + (x + dx + NX) % NX

    loads = [
        pltpu.make_async_copy(q_hbm.at[pl.ds(HALF, HALF), :], qin.at[2], load_sem.at[0]),
        pltpu.make_async_copy(k_hbm, kv.at[0, s], load_sem.at[1]),
        pltpu.make_async_copy(v_hbm, kv.at[1, s], load_sem.at[2]),
        pltpu.make_async_copy(q_hbm.at[pl.ds(0, HALF), :], qin.at[0], load_sem.at[3]),
    ]
    for load in loads:
        load.start()

    barrier = pltpu.get_barrier_semaphore()
    for dz, dx in ((0, 1), (0, -1), (1, 0), (-1, 0)):
        pl.semaphore_signal(barrier, inc=1, device_id=(at(dz, dx), t), device_id_type=MESH)
    for j in range(1, 8):
        pl.semaphore_signal(barrier, inc=1, device_id=(s, (t + j) % 8), device_id_type=MESH)
    for j in range(8):
        pl.semaphore_signal(barrier, inc=1, device_id=(mirror, j), device_id_type=MESH)
    pl.semaphore_wait(barrier, 19)

    def remote_q():
        return pltpu.make_async_remote_copy(
            src_ref=qin.at[2], dst_ref=qin.at[1], send_sem=qsend, recv_sem=qrecv,
            device_id=(mirror, t), device_id_type=MESH,
        )

    def block_copy(which, block, part, lane, device):
        rows = pl.ds(0, BLK) if part == 2 else pl.ds(part * HALF, HALF)
        return pltpu.make_async_remote_copy(
            src_ref=kv.at[which, block, rows, :],
            dst_ref=kv.at[which, block, rows, :],
            send_sem=send_sem.at[which, block, lane],
            recv_sem=recv_sem.at[which, block, part % 2],
            device_id=(device, t), device_id_type=MESH,
        )

    lanes = ((0, 1), (0, -1), (1, 0), (-1, 0))

    def sends(which, d):
        first = which
        dz, dx = d
        near, far = (dx, dz) if first == 0 else (dz, dx)
        near_lanes, far_lanes = ((0, 1), (2, 3)) if first == 0 else ((2, 3), (0, 1))
        if d == (0, 0):
            return [(2, near_lanes[0]), (2, near_lanes[1]), (2, far_lanes[0]), (2, far_lanes[1])]
        if far == 0:
            out = [(2, far_lanes[0]), (2, far_lanes[1])]
            if near == -1:
                out = [(0, near_lanes[0])] + out
            if near == 1:
                out = [(1, near_lanes[1])] + out
            return out
        if far == -1:
            return [(0, far_lanes[0])]
        if far == 1:
            return [(1, far_lanes[1])]
        return []

    def halves(which, d):
        dz, dx = d
        near, far = (dx, dz) if which == 0 else (dz, dx)
        return far == 2 or (far == 0 and near == 2)

    def pass_on(which, d):
        block = at(*d)
        for part, lane in sends(which, d):
            block_copy(which, block, part, lane, at(*lanes[lane])).start()

    def arrive(which, d):
        block = at(*d)
        for part in (0, 1) if halves(which, d) else (2,):
            block_copy(which, block, part, 0, s).wait_recv()

    loads[0].wait()
    remote_q().start()
    loads[1].wait()
    loads[2].wait()
    own_k, own_v = sends(0, (0, 0)), sends(1, (0, 0))
    for which, part, lane in (
        [(0,) + own_k[0], (0,) + own_k[1], (1,) + own_v[0], (1,) + own_v[1]]
        + [(0,) + own_k[2], (0,) + own_k[3], (1,) + own_v[2], (1,) + own_v[3]]
    ):
        block_copy(which, s, part, lane, at(*lanes[lane])).start()
    loads[3].wait()

    mx[...] = jnp.full(mx.shape, -1e30, jnp.float32)
    acc[...] = jnp.zeros(acc.shape, jnp.float32)
    lane_ids = lax.broadcasted_iota(jnp.int32, (HALF, 2 * DH), 1)

    def split_maps(half):
        q = qin[half]
        zero = jnp.zeros_like(q)
        qs[half, 0] = jnp.where(lane_ids < DH, q, zero)
        qs[half, 1] = jnp.where(lane_ids < DH, zero, q)

    split_maps(0)
    remote_q().wait_recv()
    split_maps(1)

    scale = LOG2E * DH ** (-0.5)
    TQ = 256

    def tiles(half, block, masked):
        k = kv[0, block]
        v = kv[1, block]
        ones = jnp.ones_like(v)
        vv = jnp.concatenate([v, ones], axis=1)
        for m in range(2):
            for r in range(HALF // TQ):
                rows = pl.ds(r * TQ, TQ)
                scores = lax.dot_general(
                    qs[half, m, rows, :], k, (((1,), (1,)), ((), ())),
                    preferred_element_type=jnp.float32,
                ) * scale
                if masked:
                    row_id = lax.broadcasted_iota(jnp.int32, scores.shape, 0) + (half * HALF + r * TQ)
                    col_id = lax.broadcasted_iota(jnp.int32, scores.shape, 1)
                    scores = jnp.where(col_id <= row_id, scores, -1e30)
                old = mx[half, m, rows, :]
                new = jnp.maximum(old, jnp.max(scores, axis=1, keepdims=True))
                factor = jnp.exp2(old - new)
                wide = jnp.concatenate([new] * (BLK // 128), axis=1)
                weights = jnp.exp2(scores - wide).astype(jnp.bfloat16)
                pv = jnp.dot(weights, vv, preferred_element_type=jnp.float32)
                mx[half, m, rows, :] = new
                acc[half, m, rows, :] = acc[half, m, rows, :] * jnp.concatenate([factor, factor], axis=1) + pv

    def step(i, carry):
        for k, events in EVENTS.items():
            @pl.when(i == k)
            def _(events=events):
                for kd, vd in events:
                    arrive(0, kd)
                    pass_on(0, kd)
                    arrive(1, vd)
                    pass_on(1, vd)

        dz = jnp.int32(0)
        dx = jnp.int32(0)
        for k, (a, b) in enumerate(ORDER):
            dz = jnp.where(i == k, a, dz)
            dx = jnp.where(i == k, b, dx)
        block = at(dz, dx)

        def one_half(half, c):
            limit = jnp.where(half == 0, s, mirror)

            @pl.when(block < limit)
            def _():
                tiles(half, block, False)

            @pl.when(block == limit)
            def _():
                tiles(half, block, True)

            return c

        return lax.fori_loop(0, 2, one_half, carry)

    lax.fori_loop(0, NZ * NX, step, 0)

    lam = lam_ref[0]
    gain = gain_ref[...]
    for half in range(2):
        for r in range(HALF // 128):
            rows = pl.ds(r * 128, 128)
            mixed = [acc[half, m, rows, :128] / acc[half, m, rows, 128:] for m in range(2)]
            contrast = mixed[0] - lam * mixed[1]
            mean = jnp.mean(contrast * contrast, axis=1, keepdims=True)
            obuf[half, rows, :] = (contrast * lax.rsqrt(mean + 1e-05) * gain).astype(jnp.bfloat16)
    columns = pl.ds(pl.multiple_of(t * 128, 128), 128)

    def out_copy(half, j, sender):
        rows = pl.ds(j * 128, 128)
        cols = pl.ds(pl.multiple_of(sender * 128, 128), 128)
        return pltpu.make_async_remote_copy(
            src_ref=obuf.at[half, rows, :], dst_ref=out_ref.at[:, cols],
            send_sem=osend.at[half, j], recv_sem=orecv.at[sender],
            device_id=(s if half == 0 else mirror, 4 * half + j), device_id_type=MESH,
        )

    for j in range(4):
        out_copy(1, j, t).start()
        @pl.when(t != j)
        def _():
            out_copy(0, j, t).start()
        @pl.when(t == j)
        def _():
            out_ref[:, columns] = obuf[0, j * 128:(j + 1) * 128, :]
    for j in range(8):
        @pl.when(jnp.logical_or(t >= 4, t != j))
        def _():
            out_copy(0, 0, j).wait_recv()
    for j in range(4):
        out_copy(1, j, t).wait_send()
        @pl.when(t != j)
        def _():
            out_copy(0, j, t).wait_send()
    remote_q().wait_send()
    for which in range(2):
        for d in ORDER:
            for part, lane in sends(which, d):
                block_copy(which, at(*d), part, lane, s).wait_send()


def attention(lambdas, head_gain, queries, key_rows, value_rows):
    any_space = pl.BlockSpec(memory_space=pl.ANY)
    return pl.pallas_call(
        attention_kernel,
        out_shape=jax.ShapeDtypeStruct((128, 1024), jnp.bfloat16),
        in_specs=[
            pl.BlockSpec(memory_space=pltpu.SMEM),
            pl.BlockSpec(memory_space=pltpu.VMEM),
            any_space, any_space, any_space,
        ],
        out_specs=pl.BlockSpec(memory_space=pltpu.VMEM),
        scratch_shapes=[
            pltpu.VMEM((2, NZ * NX, BLK, 128), jnp.bfloat16),
            pltpu.VMEM((3, HALF, 128), jnp.bfloat16),
            pltpu.VMEM((2, 2, HALF, 128), jnp.bfloat16),
            pltpu.VMEM((2, 2, HALF, 128), jnp.float32),
            pltpu.VMEM((2, 2, HALF, 256), jnp.float32),
            pltpu.VMEM((2, HALF, 128), jnp.bfloat16),
            pltpu.SemaphoreType.DMA((4,)),
            pltpu.SemaphoreType.DMA,
            pltpu.SemaphoreType.DMA,
            pltpu.SemaphoreType.DMA((2, NZ * NX, 4)),
            pltpu.SemaphoreType.DMA((2, NZ * NX, 2)),
            pltpu.SemaphoreType.DMA((2, 4)),
            pltpu.SemaphoreType.DMA((8,)),
        ],
        compiler_params=pltpu.CompilerParams(
            collective_id=0, has_side_effects=True, vmem_limit_bytes=48 * 1024 * 1024
        ),
        name="attention",
    )(lambdas, head_gain.reshape(1, -1), queries, key_rows, value_rows)


def expert_rows(rows_in, gate_local, up_local, down_local):
    flat = rows_in.reshape(-1, rows_in.shape[-1])
    gate = jnp.dot(flat, gate_local, preferred_element_type=jnp.float32)
    upper = jnp.dot(flat, up_local, preferred_element_type=jnp.float32)
    act = (jax.nn.silu(gate) * upper).astype(jnp.bfloat16)
    result = jnp.dot(act, down_local, preferred_element_type=jnp.float32)
    return result.reshape(rows_in.shape)


def local(
    queries,
    key_rows,
    value_rows,
    lambdas,
    head_gain,
    out_weight,
    stream,
    ffn_gain,
    routes,
    route_weight,
    gate_weight,
    up_weight,
    down_weight,
):
    heads_local = attention(lambdas, head_gain, queries, key_rows, value_rows)
    attended = stream.astype(jnp.float32) + jnp.dot(
        heads_local, out_weight, preferred_element_type=jnp.float32
    )
    normed = (
        attended
        * lax.rsqrt(jnp.mean(attended * attended, axis=-1, keepdims=True) + 1e-06)
        * ffn_gain
    ).astype(jnp.bfloat16)
    rows_local = normed.shape[0]
    width = normed.shape[1]
    top_count = routes.shape[1]
    sp_size = lax.axis_size("sp")
    experts = sp_size * gate_weight.shape[0]
    slots = max(2, (rows_local * top_count * 5 + 4 * experts - 1) // (4 * experts))
    flat_routes = routes.reshape(-1)
    onehot = (flat_routes[:, None] == jnp.arange(experts, dtype=jnp.int32)[None, :]).astype(
        jnp.int32
    )
    before = jnp.cumsum(onehot, axis=0) - onehot
    slot = jnp.sum(before * onehot, axis=1)
    target = flat_routes * slots + slot
    placed = (target[:, None] == jnp.arange(experts * slots, dtype=jnp.int32)[None, :]).astype(
        jnp.float32
    )
    placed = placed.reshape(rows_local, top_count, experts * slots)
    dispatch = jnp.transpose(jnp.sum(placed, axis=1)).astype(jnp.bfloat16)
    combine = jnp.einsum("tk,tks->ts", route_weight, placed)
    outgoing = (
        jnp.dot(dispatch, normed, preferred_element_type=jnp.float32)
        .astype(jnp.bfloat16)
        .reshape(experts, slots, width)
    )
    gate_local = gate_weight[0]
    up_local = up_weight[0]
    down_local = down_weight[0]
    arrived = lax.all_to_all(outgoing, "sp", split_axis=0, concat_axis=0, tiled=True)
    partial_value = expert_rows(
        lax.all_gather(arrived[:, None], "tp", axis=1, tiled=True), gate_local, up_local, down_local
    )
    summed = lax.psum_scatter(
        partial_value.astype(jnp.bfloat16), "tp", scatter_dimension=1, tiled=True
    )
    returned = lax.all_to_all(summed, "sp", split_axis=0, concat_axis=0, tiled=True).reshape(
        experts * slots, width
    )
    routed = jnp.dot(combine, returned.astype(jnp.float32))
    return (attended + routed).astype(jnp.bfloat16)


def solution(mesh):
    placed = (
        P("sp", "tp"),
        P("sp", "tp"),
        P("sp", "tp"),
        P("tp"),
        P(),
        P(),
        P(("sp", "tp"), None),
        P(),
        P(("sp", "tp"), None),
        P(("sp", "tp"), None),
        P("sp", None, "tp"),
        P("sp", None, "tp"),
        P("sp", "tp", None),
    )
    return jax.shard_map(
        local, mesh=mesh, in_specs=placed, out_specs=P(("sp", "tp"), None), check_vma=False
    )
```

time: 608 us -> 366 us (0.60)
  blocking collectives: 264 us -> 59.6 us
  waiting for transfers between devices: 195 us -> 122 us
  Pallas kernels: 0 us -> 72.2 us
  local copies, waits for them, and re-layouts: 62.8 us -> 49.9 us
  matrix products: 52.5 us -> 43.2 us
  other arithmetic: 8.29 us -> 1.5 us
    all_to_all x1, blocking collectives: 236 us -> 31.7 us  [local(): lax.all_to_all(outgoing, 'sp', split_axis=0, concat_axis=0, tiled=True)]
    pallas_call x0 -> x1, Pallas kernels: none -> 72.2 us  [attention(): pl.pallas_call(attention_kernel, out_shape=jax.ShapeDtypeStruct((128, 102...]
    all_gather x1 -> x0, waiting for transfers between devices: 70.9 us -> none  [side_by_side(): lax.all_gather(both, axis, axis=dim, tiled=True)]
    dot_general x4 -> x0, matrix products: 9.29 us -> none  [the longest x2 7.28 us: compute(): jnp.einsum('hmqk,khe->hmqe', expo.astype(jnp.bfloat16), value_block, pref...]
    all_to_all x1 -> x0, waiting for transfers between devices: 6.37 us -> none  [local(): lax.all_to_all(heads_out, 'tp', split_axis=0, concat_axis=1, tiled=True)]
  transfers between devices with their start and end apart: 4 -> 2, of which waited for: 4 -> 2; matrix products, arithmetic and copies ran while one was open for 1% -> 0% of each run, Pallas kernels for 0% -> 0%
where the time goes in v1:
time: 366 us; the launch traced here: 363 us
  waiting for transfers between devices  122 us (33%)
  Pallas kernels  72.2 us (20%)
  blocking collectives  59.6 us (16%)
  local copies, waits for them, and re-layouts  49.9 us (14%)
  matrix products  43.2 us (12%)
  between operations  14.2 us (4%)
    pallas_call x1, Pallas kernels, attention(): pl.pallas_call(attention_kernel, out_shape=jax.ShapeDtypeStruct((128, 102...  72.2 us
    reduce_scatter x1, waiting for transfers between devices, local(): lax.psum_scatter(partial_value.astype(jnp.bfloat16), 'tp', scatter_dimens...  61.9 us
    all_gather x1, waiting for transfers between devices, local(): lax.all_gather(arrived[:, None], 'tp', axis=1, tiled=True)  60.5 us
    all_to_all x1, blocking collectives, local(): lax.all_to_all(outgoing, 'sp', split_axis=0, concat_axis=0, tiled=True)  31.7 us
    all_to_all x1, blocking collectives, local(): lax.all_to_all(summed, 'sp', split_axis=0, concat_axis=0, tiled=True)  28 us
    convert_element_type x1, local copies, waits for them, and re-layouts, local(): partial_value.astype(jnp.bfloat16)  13.9 us
    all_gather x1, local copies, waits for them, and re-layouts, local(): lax.all_gather(arrived[:, None], 'tp', axis=1, tiled=True)  13.6 us
    dot_general x1, matrix products, expert_rows(): result = jnp.dot(act, down_local, preferred_element_type=jnp.float32)  12.7 us
  transfers between devices with their start and end apart: 2, of which 2 were waited for; matrix products, arithmetic and copies ran while one was open for 0% of the time, Pallas kernels for 0%

profile of v1, /device:TPU:1, one launch (start us, length us, event | category | flops | bytes accessed | tf_op | source)
XLA Modules:
  0.0 363.4 jit_solution(18205889291120265959)
XLA Ops:
  6.5 0.0 copy-start
  6.5 0.0 copy-start.8
  6.5 0.0 copy-start.7
  6.5 0.0 all-gather.3.cloned.1.call-start
  6.5 0.9 copy.56
  7.5 0.1 eq.44
  7.6 0.1 eq.40
  8.4 0.6 reduce-window.6
  9.0 0.2 slice_reduce_fusion
  9.3 0.1 fusion.10
  9.3 0.1 reduce_sum.30
  9.5 0.1 copy.59
  9.6 0.7 multiply_add_fusion
  10.3 0.0 copy-start.1
  10.3 0.9 copy-done.1
  11.2 0.0 copy-start.2
  11.2 0.9 copy-done.2
  12.2 0.9 copy-done.3
  13.1 0.7 copy-done.4
  13.8 72.2 %attention.1 = bf16[128,1024]{1,0:T(8,128)(2,1)S(1)} custom-call(f32[1]{0:T(128)S(6)} %copy.74.lam_ref, f32[1,128]{1,0:T(1,128)S(1)} %bitcast.42, bf16[1024,128]{1,0:T(8,128)(2,1)S(1)} %copy-done.1, bf16[1024,128]{1,0:T(8,128)(2,1)S(1)} %copy-done.2, bf16[1024,128]{1,0:T(8,128)(2,1)S(1)} %copy-done.3), custom_call_target="tpu_custom_call" | custom-call | tf_op jit(solution)/shard_map/attention/pallas_call | solution.py:252
  86.0 3.1 multiply_reduce_fusion
  89.2 0.0 copy-start.6
  89.2 0.0 copy-done.8
  89.2 0.1 convert_reduce_fusion
  89.3 0.9 copy-done.6
  90.1 0.0 copy-done.7
  90.1 1.6 convolution_convert_fusion.1
  91.8 3.2 reshape.68
  95.0 31.7 %all_to_all.10 = bf16[16,20,2048]{2,1,0:T(8,128)(2,1)S(1)} all-to-all(bf16[16,20,2048]{2,1,0:T(8,128)(2,1)} %reshape.68), channel_id=1, replica_groups=mesh['sp'=16,'tp'=8] {'sp'}, dimensions={0} | all-to-all | bytes 2621440 | tf_op jit(solution)/shard_map/all_to_all | solution.py:343
  126.7 1.8 copy.60
  128.5 0.0 all-gather.3.cloned.1.call-update
  128.5 0.2 reduce-scatter.2.cloned.1.call-start
  128.7 60.5 %all-gather.3.cloned.1.call-done = bf16[16,160,2048]{2,0,1:T(8,128)(2,1)} async-done(((bf16[16,20,2048]{2,0,1:T(8,128)(2,1)}), bf16[16,160,2048]{2,0,1:T(8,128)(2,1)}) %all-gather.3.cloned.1.call-update) | async-done | bytes 10485776 | tf_op jit(solution)/shard_map/all_gather | solution.py:345
  189.2 13.6 %copy.61 = bf16[16,160,2048]{2,1,0:T(8,128)(2,1)} copy(bf16[16,160,2048]{2,0,1:T(8,128)(2,1)} %all-gather.3.cloned.1.call-done) | data formatting | bytes 20971520 | tf_op jit(solution)/shard_map/all_gather | solution.py:345
  202.8 12.4 %fusion.2 = f32[2560,640]{1,0:T(8,128)S(1)} fusion(bf16[2560,2048]{1,0:T(8,128)(2,1)} %bitcast.43, bf16[1,2048,640]{2,1,0:T(8,128)(2,1)} %param.23), kind=kOutput, calls=%fused_computation.5 | convolution fusion | flops 6710886400 | bytes 19660800 | tf_op jit(solution)/shard_map/dot_general | solution.py:285
  215.3 0.0 copy-done.5
  215.3 0.0 copy-done.9
  215.3 10.4 %multiply_convert_fusion = bf16[2560,640]{1,0:T(8,128)(2,1)} fusion(f32[2560,640]{1,0:T(8,128)S(1)} %fusion.2, bf16[2560,2048]{1,0:T(8,128)(2,1)S(1)} %bitcast.44, bf16[1,2048,640]{2,1,0:T(8,128)(2,1)S(1)} %copy-done.9), kind=kOutput, calls=%fused_computation.1 | convolution fusion | flops 6720716800 | bytes 22937600 | tf_op jit(solution)/shard_map/dot_general | solution.py:286
  225.7 6.1 %dot_general.28 = bf16[16,8,20,640]{3,2,1,0:T(8,128)(2,1)} reshape(bf16[2560,640]{1,0:T(8,128)(2,1)} %multiply_convert_fusion) | data formatting | bytes 6553600 | tf_op jit(solution)/shard_map/dot_general | solution.py:288
  231.8 0.0 copy-done
  231.8 12.7 %convolution_convert_fusion = bf16[16,8,20,2048]{3,2,1,0:T(8,128)(2,1)S(1)} fusion(bf16[16,8,20,640]{3,2,1,0:T(8,128)(2,1)} %dot_general.28, bf16[1,640,2048]{2,1,0:T(8,128)(2,1)S(1)} %copy-done), kind=kOutput, calls=%fused_computation | convolution fusion | flops 6716129280 | bytes 16384000 | tf_op jit(solution)/shard_map/dot_general | solution.py:288
  244.5 13.9 %copy.62 = bf16[16,8,20,2048]{3,0,2,1:T(8,128)(2,1)} copy(bf16[16,8,20,2048]{3,2,1,0:T(8,128)(2,1)S(1)} %convolution_convert_fusion) | data formatting | bytes 20971520 | tf_op jit(solution)/shard_map/convert_element_type | solution.py:348
  258.4 0.0 reduce-scatter.2.cloned.1.call-update
  258.4 61.9 %reduce-scatter.2.cloned.1.call-done = bf16[16,1,20,2048]{3,0,2,1:T(8,128)(2,1)} async-done(((bf16[16,8,20,2048]{3,0,2,1:T(8,128)(2,1)}), bf16[16,1,20,2048]{3,0,2,1:T(8,128)(2,1)}) %reduce-scatter.2.cloned.1.call-update) | async-done | bytes 1310736 | tf_op jit(solution)/shard_map/reduce_scatter | solution.py:347
  320.3 2.0 copy.63
  322.4 28.0 %all_to_all.11 = bf16[16,1,20,2048]{3,2,1,0:T(8,128)(2,1)} all-to-all(bf16[16,1,20,2048]{3,2,1,0:T(8,128)(2,1)S(1)} %copy.63), channel_id=1, replica_groups=mesh['sp'=16,'tp'=8] {'sp'}, dimensions={0} | all-to-all | bytes 2621440 | tf_op jit(solution)/shard_map/all_to_all | solution.py:350
  350.4 3.3 reshape.70
  353.7 2.9 fusion.4
  (8 shorter events, 0.1 us)
Async XLA Ops:
  6.5 225.3 %copy-start = (bf16[1,640,2048]{2,1,0:T(8,128)(2,1)S(1)}, bf16[1,640,2048]{2,1,0:T(8,128)(2,1)}, u32[]{:S(2)}) copy-start(bf16[1,640,2048]{2,1,0:T(8,128)(2,1)} %param.25) | copy-start | bytes 7864324
  6.5 82.6 %copy-start.8 = (f32[128,2]{0,1:T(2,128)S(1)}, f32[128,2]{0,1:T(2,128)}, u32[]{:S(2)}) copy-start(f32[128,2]{0,1:T(2,128)} %param.22) | copy-start | bytes 3076
  6.5 83.6 %copy-start.7 = (f32[2048]{0:T(1024)S(1)}, f32[2048]{0:T(1024)}, u32[]{:S(2)}) copy-start(f32[2048]{0:T(1024)} %param.20) | copy-start | bytes 24580
  6.5 182.7 %all-gather.3.cloned.1.call-start = ((), (), s32[]{:S(2)}) async-start(), calls=%async_computation.4 | async-start | bytes 11796480 | tf_op jit(solution)/shard_map/all_gather | solution.py:345
  10.3 0.9 copy-start.1
  11.2 0.9 copy-start.2
  12.2 0.9 copy-start.3
  13.1 0.7 copy-start.4
  89.2 1.0 copy-start.6
  128.5 191.9 %reduce-scatter.2.cloned.1.call-start = ((), (), s32[]{:S(2)}) async-start(), calls=%async_computation.3 | async-start | bytes 11796480 | tf_op jit(solution)/shard_map/reduce_scatter | solution.py:347
  202.8 12.5 %copy-start.5 = (bf16[16,160,2048]{2,1,0:T(8,128)(2,1)S(1)}, bf16[16,160,2048]{2,1,0:T(8,128)(2,1)}, u32[]{:S(2)}) copy-start(bf16[16,160,2048]{2,1,0:T(8,128)(2,1)} %copy.61) | copy-start | bytes 31457284
  202.8 12.5 %copy-start.9 = (bf16[1,2048,640]{2,1,0:T(8,128)(2,1)S(1)}, bf16[1,2048,640]{2,1,0:T(8,128)(2,1)}, u32[]{:S(2)}) copy-start(bf16[1,2048,640]{2,1,0:T(8,128)(2,1)} %param.24) | copy-start | bytes 7864324
Sparse Core Ops, SparseCore 0:
  128.6 60.5 all-gather.2
  258.5 61.7 reduce-scatter.1

commit v2 on v1

--- a/solution.py
+++ b/solution.py
@@ -280,13 +280,360 @@
     )(lambdas, head_gain.reshape(1, -1), queries, key_rows, value_rows)
 
 
-def expert_rows(rows_in, gate_local, up_local, down_local):
-    flat = rows_in.reshape(-1, rows_in.shape[-1])
-    gate = jnp.dot(flat, gate_local, preferred_element_type=jnp.float32)
-    upper = jnp.dot(flat, up_local, preferred_element_type=jnp.float32)
-    act = (jax.nn.silu(gate) * upper).astype(jnp.bfloat16)
-    result = jnp.dot(act, down_local, preferred_element_type=jnp.float32)
-    return result.reshape(rows_in.shape)
+GROUPS = (0, -1, 1, 2)
+MAIN = 16
+CH = 80
+WID = 2048
+HW = 1024
+REM = 512
+BAND = WID + REM
+NT = 8
+
+
+def expert_kernel(
+    heads_ref, stream_ref, gain_ref, routes_ref, rw_ref, ow_hbm, gate_hbm, up_hbm, down_hbm,
+    out_ref,
+    ow, gw, uw, dw, att, nrm, outg, arr, reto, ret, xs, act, ps, pr, rh, rf, cm, cr,
+    load_sem, psend, precv, xsend, xrecv, qsend, qrecv, rsend, rhrecv, rfrecv, bsend, brecv,
+):
+    s = lax.axis_index("sp")
+    t = lax.axis_index("tp")
+    z, x = s // NX, s % NX
+    y, c = t // 2, t % 2
+    mate = 2 * y + 1 - c
+    bf16, f32 = jnp.bfloat16, jnp.float32
+
+    def at(dz, dx):
+        return ((z + dz + NZ) % NZ) * NX + (x + dx + NX) % NX
+
+    def lane(dy, core):
+        return 2 * ((y + dy + 4) % 4) + core
+
+    loads = [
+        pltpu.make_async_copy(ow_hbm, ow, load_sem.at[0]),
+        pltpu.make_async_copy(gate_hbm.at[0], gw, load_sem.at[1]),
+        pltpu.make_async_copy(up_hbm.at[0], uw, load_sem.at[2]),
+        pltpu.make_async_copy(down_hbm.at[0], dw, load_sem.at[3]),
+    ]
+    for load in loads:
+        load.start()
+
+    barrier = pltpu.get_barrier_semaphore()
+    others = [(dz, dx) for dz in GROUPS for dx in (0, 1, -1, 2) if (dz, dx) != (0, 0)]
+    for dz, dx in others:
+        pl.semaphore_signal(barrier, inc=1, device_id=(at(dz, dx), t), device_id_type=MESH)
+    for peer in (lane(1, c), lane(-1, c), mate):
+        pl.semaphore_signal(barrier, inc=1, device_id=(s, peer), device_id_type=MESH)
+
+    loads[0].wait()
+    heads = heads_ref[...]
+    square = jnp.zeros((128, 1), f32)
+    for k in range(0, WID, 512):
+        cols = pl.ds(k, 512)
+        value = stream_ref[:, cols].astype(f32) + jnp.dot(heads, ow[:, cols], preferred_element_type=f32)
+        att[:, cols] = value
+        square = square + jnp.sum(value * value, axis=1, keepdims=True)
+    inverse = lax.rsqrt(square * (1.0 / WID) + 1e-06)
+    for k in range(0, WID, 512):
+        cols = pl.ds(k, 512)
+        nrm[:, cols] = (att[:, cols] * inverse * gain_ref[:, cols]).astype(bf16)
+
+    experts = lax.broadcasted_iota(jnp.int32, (128, 16), 1)
+    route = [routes_ref[:, k:k + 1] for k in range(2)]
+    hot = [(r == experts).astype(f32) for r in route]
+    row_id = lax.broadcasted_iota(jnp.int32, (128, 128), 0)
+    col_id = lax.broadcasted_iota(jnp.int32, (128, 128), 1)
+    earlier = (col_id < row_id).astype(f32).astype(bf16)
+    before = jnp.dot(earlier, (hot[0] + hot[1]).astype(bf16), preferred_element_type=f32)
+    place = lax.broadcasted_iota(jnp.int32, (128, 256), 1).astype(f32)
+    main_hit, rem_hit = [], []
+    for k in range(2):
+        slot = jnp.sum(before * hot[k], axis=1, keepdims=True)
+        base = route[k].astype(f32) * 16.0 + slot
+        low = slot < float(MAIN)
+        main_hit.append((jnp.where(low, base, -1.0) == place).astype(f32))
+        rem_hit.append([
+            (jnp.where(low, -1.0, base + (4.0 * j - 16.0)) == place).astype(f32) for j in range(4)
+        ])
+    weight = [rw_ref[:, k:k + 1] for k in range(2)]
+    over_rows = (((0,), (0,)), ((), ()))
+    chosen = (main_hit[0] + main_hit[1]).astype(bf16)
+    for k in range(0, WID, 512):
+        cols = pl.ds(k, 512)
+        outg[:, cols] = lax.dot_general(
+            chosen, nrm[:, cols], over_rows, preferred_element_type=f32
+        ).astype(bf16)
+    extra = jnp.zeros((256, REM), f32)
+    for j in range(4):
+        extra = extra + lax.dot_general(
+            (rem_hit[0][j] + rem_hit[1][j]).astype(bf16), nrm[:, pl.ds(j * REM, REM)], over_rows,
+            preferred_element_type=f32,
+        )
+    outg[:, pl.ds(WID, REM)] = extra.astype(bf16)
+
+    def keep_split(ref, value):
+        high = value.astype(bf16)
+        ref[:, pl.ds(0, 256)] = high
+        ref[:, pl.ds(256, 256)] = (value - high.astype(f32)).astype(bf16)
+
+    pl.semaphore_wait(barrier, len(others) + 3)
+
+    def band(device):
+        return pl.ds(pl.multiple_of(device * MAIN, MAIN), MAIN)
+
+    def plane_copy(source, target, ssem, rsem, to, sender):
+        return pltpu.make_async_remote_copy(
+            src_ref=source.at[band(to), :], dst_ref=target.at[band(sender), :],
+            send_sem=ssem.at[to], recv_sem=rsem.at[sender],
+            device_id=(to, t), device_id_type=MESH,
+        )
+
+    for dz, dx in others:
+        plane_copy(outg, arr, psend, precv, at(-dz, -dx), s).start()
+    arr[band(s), :] = outg[band(s), :]
+    keep_split(cm, weight[0] * main_hit[0] + weight[1] * main_hit[1])
+    for j in range(4):
+        keep_split(cr.at[j], weight[0] * rem_hit[0][j] + weight[1] * rem_hit[1][j])
+
+    fold_row = lax.broadcasted_iota(jnp.int32, (16, 64), 0)
+    fold_col = lax.broadcasted_iota(jnp.int32, (16, 64), 1)
+    fold = [
+        (fold_col == 16 * (fold_row >> 2) + 4 * j + (fold_row & 3)).astype(f32).astype(bf16)
+        for j in range(4)
+    ]
+
+    def rows_of(position):
+        return pl.ds(pl.multiple_of(position * CH, 16), CH)
+
+    def x_copy(g, position, part, send, to, slot=None):
+        cols = pl.ds(0, WID) if part == 2 else pl.ds(part * HW, HW)
+        return pltpu.make_async_remote_copy(
+            src_ref=xs.at[g, rows_of(position), cols], dst_ref=xs.at[g, rows_of(position), cols],
+            send_sem=xsend.at[g, send], recv_sem=xrecv.at[g, position, part % 2],
+            device_id=(s, to), device_id_type=MESH,
+        )
+
+    def x_sends(g):
+        return [
+            (g, t, 2, 0, lane(1, c)), (g, t, 2, 1, lane(-1, c)), (g, t, 2, 2, mate),
+            (g, lane(-1, c), 0, 3, lane(1, c)), (g, lane(-1, c), 2, 4, mate),
+            (g, lane(1, c), 1, 5, lane(-1, c)), (g, lane(1, c), 2, 6, mate),
+            (g, lane(2, c), 2, 7, mate),
+        ]
+
+    def group_rows(g):
+        zz = (z + GROUPS[g] + NZ) % NZ
+        return pl.ds(pl.multiple_of(zz * 64, 64), 64)
+
+    def build(g):
+        for dx in (0, 1, -1, 2):
+            if (GROUPS[g], dx) != (0, 0):
+                plane_copy(outg, arr, psend, precv, s, at(GROUPS[g], dx)).wait_recv()
+        rows = group_rows(g)
+        first = pl.multiple_of(t * CH, 16)
+        for k in range(0, WID, 512):
+            xs[g, pl.ds(first, 64), pl.ds(k, 512)] = arr[rows, pl.ds(k, 512)]
+        for j in range(4):
+            xs[g, pl.ds(first + 64, 16), pl.ds(j * REM, REM)] = jnp.dot(
+                fold[j], arr[rows, pl.ds(WID, REM)], preferred_element_type=f32
+            ).astype(bf16)
+        for copy in x_sends(g)[:3]:
+            x_copy(*copy).start()
+
+    def forward(g):
+        todo = x_sends(g)
+        x_copy(g, lane(-1, c), 2, 0, t).wait_recv()
+        x_copy(*todo[3]).start()
+        x_copy(*todo[4]).start()
+        x_copy(g, lane(1, c), 2, 0, t).wait_recv()
+        x_copy(*todo[5]).start()
+        x_copy(*todo[6]).start()
+
+    def far(g):
+        x_copy(g, lane(2, c), 0, 0, t).wait_recv()
+        x_copy(g, lane(2, c), 1, 0, t).wait_recv()
+        x_copy(*x_sends(g)[7]).start()
+
+    def pair_copy(g, yy):
+        return pltpu.make_async_remote_copy(
+            src_ref=ps.at[g, rows_of(2 * yy + 1 - c), :], dst_ref=pr.at[g, yy],
+            send_sem=qsend.at[g, yy], recv_sem=qrecv.at[g, yy],
+            device_id=(s, mate), device_id_type=MESH,
+        )
+
+    TURN = (2, 1, 3, 0)
+
+    def compute(g):
+        for dy in (0, -1, 1, 2):
+            x_copy(g, lane(dy, 1 - c), 2, 0, t).wait_recv()
+        if g == 0:
+            for load in loads[1:]:
+                load.wait()
+
+        def block(i, carry):
+            dy = jnp.where(i == 0, 2, jnp.where(i == 1, 1, jnp.where(i == 2, 3, 0)))
+            yy = (y + dy) % 4
+            rows = pl.ds(pl.multiple_of(yy * 2 * CH, 32), 2 * CH)
+            value = xs[g, rows, :]
+            gate = jnp.dot(value, gw[...], preferred_element_type=f32)
+            upper = jnp.dot(value, uw[...], preferred_element_type=f32)
+            act[...] = (gate / (1.0 + jnp.exp(-gate)) * upper).astype(bf16)
+            ps[g, rows, :] = jnp.dot(act[...], dw[...], preferred_element_type=f32).astype(bf16)
+            pair_copy(g, yy).start()
+            return carry
+
+        lax.fori_loop(0, 4, block, 0)
+
+    def add_into(g, position, cols, terms):
+        rows = rows_of(position)
+        total = ps[g, rows, cols].astype(f32)
+        for term in terms:
+            total = total + term.astype(f32)
+        ps[g, rows, cols] = total.astype(bf16)
+
+    def r_copy(g, dy, part, send, direction, ref, sem, slot):
+        cols = pl.ds(part * HW, HW)
+        return pltpu.make_async_remote_copy(
+            src_ref=ps.at[g, rows_of(lane(dy, c)), cols], dst_ref=ref.at[(g,) + slot],
+            send_sem=rsend.at[g, send], recv_sem=sem.at[(g,) + slot],
+            device_id=(s, lane(direction, c)), device_id_type=MESH,
+        )
+
+    def r_sends(g):
+        return [
+            (g, 2, 0, 0, 1, rh, rhrecv, (0,)), (g, 2, 1, 1, -1, rh, rhrecv, (1,)),
+            (g, 1, 1, 2, 1, rf, rfrecv, (0, 1)), (g, -1, 0, 3, -1, rf, rfrecv, (1, 0)),
+            (g, 1, 0, 4, 1, rf, rfrecv, (0, 0)), (g, -1, 1, 5, -1, rf, rfrecv, (1, 1)),
+        ]
+
+    def pair(g):
+        todo = r_sends(g)
+        for turn, dy in enumerate(TURN):
+            yy = (y + dy) % 4
+            pair_copy(g, yy).wait_recv()
+            for k in range(2):
+                cols = pl.ds(k * HW, HW)
+                add_into(g, 2 * yy + c, cols, [pr[g, yy, :, cols]])
+            if turn == 0:
+                r_copy(*todo[0]).start()
+                r_copy(*todo[1]).start()
+            if turn == 1:
+                r_copy(*todo[2]).start()
+            if turn == 2:
+                r_copy(*todo[3]).start()
+
+    def middle(g):
+        todo = r_sends(g)
+        r_copy(*todo[0]).wait_recv()
+        add_into(g, lane(1, c), pl.ds(0, HW), [rh[g, 0]])
+        r_copy(*todo[4]).start()
+        r_copy(*todo[1]).wait_recv()
+        add_into(g, lane(-1, c), pl.ds(HW, HW), [rh[g, 1]])
+        r_copy(*todo[5]).start()
+
+    def finish(g):
+        todo = r_sends(g)
+        for k in range(2, 6):
+            r_copy(*todo[k]).wait_recv()
+        rows = group_rows(g)
+        own = pl.multiple_of(t * CH, 16)
+        extra = jnp.zeros((64, REM), f32)
+        for j in range(4):
+            cols = pl.ds(j * REM, REM)
+            inner = pl.ds((j % 2) * REM, REM)
+            total = (
+                ps[g, pl.ds(own, CH), cols].astype(f32)
+                + rf[g, 0, j // 2, :, inner].astype(f32)
+                + rf[g, 1, j // 2, :, inner].astype(f32)
+            ).astype(bf16)
+            reto[rows, cols] = total[:64]
+            extra = extra + lax.dot_general(fold[j], total[64:], over_rows, preferred_element_type=f32)
+        reto[rows, pl.ds(WID, REM)] = extra.astype(bf16)
+        for dx in (0, 1, -1, 2):
+            to = at(GROUPS[g], dx)
+            if (GROUPS[g], dx) == (0, 0):
+                ret[band(s), :] = reto[band(s), :]
+            else:
+                plane_copy(reto, ret, bsend, brecv, to, s).start()
+
+    for stage, g in (
+        (build, 0), (build, 1), (forward, 0), (build, 2), (forward, 1), (build, 3), (far, 0),
+        (compute, 0), (pair, 0), (forward, 2), (far, 1), (compute, 1), (pair, 1), (middle, 0),
+        (forward, 3), (far, 2), (compute, 2), (pair, 2), (finish, 0), (middle, 1), (far, 3),
+        (compute, 3), (pair, 3), (middle, 2), (finish, 1), (middle, 3), (finish, 2), (finish, 3),
+    ):
+        stage(g)
+
+    for dz, dx in others:
+        plane_copy(reto, ret, bsend, brecv, s, at(dz, dx)).wait_recv()
+    for j in range(4):
+        cols = pl.ds(j * REM, REM)
+        back = ret[:, cols]
+        tail = ret[:, pl.ds(WID, REM)]
+        routed = jnp.dot(cm[...], jnp.concatenate([back, back], axis=0), preferred_element_type=f32)
+        routed = routed + jnp.dot(
+            cr[j], jnp.concatenate([tail, tail], axis=0), preferred_element_type=f32
+        )
+        out_ref[:, cols] = (att[:, cols] + routed).astype(bf16)
+
+    for dz, dx in others:
+        plane_copy(outg, arr, psend, precv, at(dz, dx), s).wait_send()
+        plane_copy(reto, ret, bsend, brecv, at(dz, dx), s).wait_send()
+    for g in range(4):
+        for copy in x_sends(g):
+            x_copy(*copy).wait_send()
+        for yy in range(4):
+            pair_copy(g, yy).wait_send()
+        for copy in r_sends(g):
+            r_copy(*copy).wait_send()
+
+
+def routed_experts(
+    heads, stream, ffn_gain, routes, route_weight, out_weight, gate_weight, up_weight, down_weight
+):
+    any_space = pl.BlockSpec(memory_space=pl.ANY)
+    vmem = pl.BlockSpec(memory_space=pltpu.VMEM)
+    bf16, f32 = jnp.bfloat16, jnp.float32
+    dma = pltpu.SemaphoreType.DMA
+    return pl.pallas_call(
+        expert_kernel,
+        out_shape=jax.ShapeDtypeStruct((128, WID), bf16),
+        in_specs=[vmem] * 5 + [any_space] * 4,
+        out_specs=vmem,
+        scratch_shapes=[
+            pltpu.VMEM((1024, WID), bf16),
+            pltpu.VMEM((WID, 640), bf16),
+            pltpu.VMEM((WID, 640), bf16),
+            pltpu.VMEM((640, WID), bf16),
+            pltpu.VMEM((128, WID), f32),
+            pltpu.VMEM((128, WID), bf16),
+            pltpu.VMEM((256, BAND), bf16),
+            pltpu.VMEM((256, BAND), bf16),
+            pltpu.VMEM((256, BAND), bf16),
+            pltpu.VMEM((256, BAND), bf16),
+            pltpu.VMEM((4, NT * CH, WID), bf16),
+            pltpu.VMEM((2 * CH, 640), bf16),
+            pltpu.VMEM((4, NT * CH, WID), bf16),
+            pltpu.VMEM((4, 4, CH, WID), bf16),
+            pltpu.VMEM((4, 2, CH, HW), bf16),
+            pltpu.VMEM((4, 2, 2, CH, HW), bf16),
+            pltpu.VMEM((128, 512), bf16),
+            pltpu.VMEM((4, 128, 512), bf16),
+            dma((4,)),
+            dma((16,)), dma((16,)),
+            dma((4, 8)), dma((4, 8, 2)),
+            dma((4, 4)), dma((4, 4)),
+            dma((4, 6)), dma((4, 2)), dma((4, 2, 2)),
+            dma((16,)), dma((16,)),
+        ],
+        compiler_params=pltpu.CompilerParams(
+            collective_id=1, has_side_effects=True, vmem_limit_bytes=63 * 1024 * 1024
+        ),
+        name="experts",
+    )(
+        heads, stream, ffn_gain.reshape(1, -1), routes, route_weight,
+        out_weight, gate_weight, up_weight, down_weight,
+    )
 
 
 def local(
@@ -305,53 +652,10 @@
     down_weight,
 ):
     heads_local = attention(lambdas, head_gain, queries, key_rows, value_rows)
-    attended = stream.astype(jnp.float32) + jnp.dot(
-        heads_local, out_weight, preferred_element_type=jnp.float32
+    return routed_experts(
+        heads_local, stream, ffn_gain, routes, route_weight,
+        out_weight, gate_weight, up_weight, down_weight,
     )
-    normed = (
-        attended
-        * lax.rsqrt(jnp.mean(attended * attended, axis=-1, keepdims=True) + 1e-06)
-        * ffn_gain
-    ).astype(jnp.bfloat16)
-    rows_local = normed.shape[0]
-    width = normed.shape[1]
-    top_count = routes.shape[1]
-    sp_size = lax.axis_size("sp")
-    experts = sp_size * gate_weight.shape[0]
-    slots = max(2, (rows_local * top_count * 5 + 4 * experts - 1) // (4 * experts))
-    flat_routes = routes.reshape(-1)
-    onehot = (flat_routes[:, None] == jnp.arange(experts, dtype=jnp.int32)[None, :]).astype(
-        jnp.int32
-    )
-    before = jnp.cumsum(onehot, axis=0) - onehot
-    slot = jnp.sum(before * onehot, axis=1)
-    target = flat_routes * slots + slot
-    placed = (target[:, None] == jnp.arange(experts * slots, dtype=jnp.int32)[None, :]).astype(
-        jnp.float32
-    )
-    placed = placed.reshape(rows_local, top_count, experts * slots)
-    dispatch = jnp.transpose(jnp.sum(placed, axis=1)).astype(jnp.bfloat16)
-    combine = jnp.einsum("tk,tks->ts", route_weight, placed)
-    outgoing = (
-        jnp.dot(dispatch, normed, preferred_element_type=jnp.float32)
-        .astype(jnp.bfloat16)
-        .reshape(experts, slots, width)
-    )
-    gate_local = gate_weight[0]
-    up_local = up_weight[0]
-    down_local = down_weight[0]
-    arrived = lax.all_to_all(outgoing, "sp", split_axis=0, concat_axis=0, tiled=True)
-    partial_value = expert_rows(
-        lax.all_gather(arrived[:, None], "tp", axis=1, tiled=True), gate_local, up_local, down_local
-    )
-    summed = lax.psum_scatter(
-        partial_value.astype(jnp.bfloat16), "tp", scatter_dimension=1, tiled=True
-    )
-    returned = lax.all_to_all(summed, "sp", split_axis=0, concat_axis=0, tiled=True).reshape(
-        experts * slots, width
-    )
-    routed = jnp.dot(combine, returned.astype(jnp.float32))
-    return (attended + routed).astype(jnp.bfloat16)
 
 
 def solution(mesh):

time: 366 us -> 206 us (0.56)
  Pallas kernels: 72.2 us -> 196 us
  waiting for transfers between devices: 122 us -> 0 us
  blocking collectives: 59.6 us -> 0 us
  matrix products: 43.2 us -> 0 us
  local copies, waits for them, and re-layouts: 49.9 us -> 8.9 us
  between operations: 14.2 us -> 0.68 us
    pallas_call x0 -> x1, Pallas kernels: none -> 124 us  [routed_experts(): pl.pallas_call(expert_kernel, out_shape=jax.ShapeDtypeStruct((128, WID),...]
    reduce_scatter x1 -> x0, waiting for transfers between devices: 61.9 us -> none  [local(): lax.psum_scatter(partial_value.astype(jnp.bfloat16), 'tp', scatter_dimens...]
    all_gather x1 -> x0, waiting for transfers between devices: 60.5 us -> none  [local(): lax.all_gather(arrived[:, None], 'tp', axis=1, tiled=True)]
    all_to_all x2 -> x0, blocking collectives: 59.6 us -> none  [the longest x1 31.7 us: local(): lax.all_to_all(outgoing, 'sp', split_axis=0, concat_axis=0, tiled=True)]
    dot_general x6 -> x0, matrix products: 43.2 us -> none  [the longest x1 12.7 us: expert_rows(): result = jnp.dot(act, down_local, preferred_element_type=jnp.float32)]
    convert_element_type x1 -> x0, local copies, waits for them, and re-layouts: 13.9 us -> none  [local(): partial_value.astype(jnp.bfloat16)]
    all_gather x1 -> x0, local copies, waits for them, and re-layouts: 13.6 us -> none  [local(): lax.all_gather(arrived[:, None], 'tp', axis=1, tiled=True)]
    reshape x2 -> x0, local copies, waits for them, and re-layouts: 6.49 us -> none  [the longest x1 3.27 us: local(): lax.all_to_all(summed, 'sp', split_axis=0, concat_axis=0, tiled=True)]
  transfers between devices with their start and end apart: 2 -> 0, of which waited for: 2 -> 0; matrix products, arithmetic and copies ran while one was open for 0% -> 0% of each run, Pallas kernels for 0% -> 0%
where the time goes in v2:
time: 206 us; the launch traced here: 205 us
  Pallas kernels  196 us (95%)
  local copies, waits for them, and re-layouts  8.9 us (4%)
    pallas_call x1, Pallas kernels, routed_experts(): pl.pallas_call(expert_kernel, out_shape=jax.ShapeDtypeStruct((128, WID),...  124 us
    pallas_call x1, Pallas kernels, attention(): pl.pallas_call(attention_kernel, out_shape=jax.ShapeDtypeStruct((128, 102...  72.2 us
    unnamed x13, local copies, waits for them, and re-layouts  8.9 us

profile of v2, /device:TPU:1, one launch (start us, length us, event | category | flops | bytes accessed | tf_op | source)
XLA Modules:
  0.0 205.4 jit_solution(10292916075903132120)
XLA Ops:
  0.7 1.4 copy.14.routes_ref
  2.1 1.4 copy.15.rw_ref
  3.5 0.0 copy-start.1
  3.5 0.9 copy-done.1
  4.4 0.0 copy-start.2
  4.4 0.9 copy-done.2
  5.4 0.0 copy-start.3
  5.4 0.9 copy-done.3
  6.3 0.0 copy-start.4
  6.3 0.7 copy-done.4
  7.0 72.2 %attention.1.heads_ref = bf16[128,1024]{1,0:T(8,128)(2,1)S(1)} custom-call(f32[1]{0:T(128)S(6)} %copy.17.lam_ref, f32[1,128]{1,0:T(1,128)S(1)} %bitcast.2, bf16[1024,128]{1,0:T(8,128)(2,1)S(1)} %copy-done.1, bf16[1024,128]{1,0:T(8,128)(2,1)S(1)} %copy-done.2, bf16[1024,128]{1,0:T(8,128)(2,1)S(1)} %copy-done.3), custom_call_target="tpu_custom_call" | custom-call | tf_op jit(solution)/shard_map/attention/pallas_call | solution.py:252
  79.2 0.0 copy-start
  79.2 0.7 copy-done
  79.9 123.6 %experts.1 = bf16[128,2048]{1,0:T(8,128)(2,1)} custom-call(bf16[128,1024]{1,0:T(8,128)(2,1)} %copy-done, bf16[128,2048]{1,0:T(8,128)(2,1)} %stream_ref.1, f32[1,2048]{1,0:T(1,128)} %bitcast.3, s32[128,2]{1,0:T(8,128)} %copy.14.routes_ref, f32[128,2]{1,0:T(8,128)} %copy.15.rw_ref, bf16[1024,2048]{1,0:T(8,128)(2,1)} %ow_hbm.1, bf16[1,2048,640]{2,1,0:T(8,128)(2,1)} %gate_hbm.1, ...), custom_call_target="tpu_custom_call" | custom-call | tf_op jit(solution)/shard_map/experts/pallas_call | solution.py:598
  203.5 1.9 copy.18
Async XLA Ops:
  3.5 0.9 copy-start.1
  4.4 0.9 copy-start.2
  5.4 0.9 copy-start.3
  6.3 0.7 copy-start.4
  79.2 0.7 copy-start

commit v3 on v2

--- a/solution.py
+++ b/solution.py
@@ -1,3 +1,5 @@
+import functools
+
 import jax
 import jax.numpy as jnp
 from jax import lax
@@ -14,241 +16,356 @@
 NX = 4
 BLK = 1024
 HALF = 512
-ORDER = (
-    (0, 0), (0, -1), (0, 1), (-1, 0), (1, 0), (-1, -1), (-1, 1), (1, -1), (1, 1),
-    (0, 2), (2, 0), (-1, 2), (2, -1), (1, 2), (2, 1), (2, 2),
+NEG = -1e30
+VROWS = 144
+TQ = 512
+KB = 256
+WORK = (
+    (0, 0), (3, 0), (1, 0), (3, 3), (1, 3), (3, 1), (1, 1),
+    (2, 0), (2, 3), (2, 1), (2, 2), (3, 2), (1, 2), (0, 3), (0, 1), (0, 2),
 )
-EVENTS = {
-    1: [((0, -1), (-1, 0)), ((0, 1), (1, 0)), ((-1, 0), (0, -1)), ((1, 0), (0, 1))],
-    3: [((0, 2), (2, 0))],
-    5: [((-1, -1), (-1, -1)), ((1, -1), (-1, 1))],
-    6: [((-1, 1), (1, -1)), ((1, 1), (1, 1))],
-    9: [((2, 0), (0, 2))],
-    10: [((-1, 2), (2, -1)), ((1, 2), (2, 1))],
-    11: [((2, -1), (-1, 2))],
-    13: [((2, 1), (1, 2))],
-    15: [((2, 2), (2, 2))],
-}
 
 
 def attention_kernel(
     lam_ref, gain_ref, q_hbm, k_hbm, v_hbm, out_ref,
-    kv, qin, qs, mx, acc, obuf,
-    load_sem, qsend, qrecv, send_sem, recv_sem, osend, orecv,
+    vin, lamv, qfull, qother, kb, vb, qm, mx, acc, pout, pin, sout, sin, obuf, sbuf0, sbuf1, fbuf0, fbuf1, nbuf0, nbuf1,
+    load_sem, lsend, lrecv, send_sem, recv_sem, msend, mrecv, psend, precv, ssend, srecv, osend, orecv,
 ):
-    s = lax.axis_index("sp")
+    sp = lax.axis_index("sp")
     t = lax.axis_index("tp")
-    z, x = s // NX, s % NX
-    mirror = NZ * NX - 1 - s
+    z, x = sp // NX, sp % NX
+    y, c = t // 2, t % 2
+    mate = 2 * y + 1 - c
+    f32, bf16 = jnp.float32, jnp.bfloat16
+    sbuf, fbuf, nbuf = (sbuf0, sbuf1), (fbuf0, fbuf1), (nbuf0, nbuf1)
 
     def at(dz, dx):
         return ((z + dz + NZ) % NZ) * NX + (x + dx + NX) % NX
 
     loads = [
-        pltpu.make_async_copy(q_hbm.at[pl.ds(HALF, HALF), :], qin.at[2], load_sem.at[0]),
-        pltpu.make_async_copy(k_hbm, kv.at[0, s], load_sem.at[1]),
-        pltpu.make_async_copy(v_hbm, kv.at[1, s], load_sem.at[2]),
-        pltpu.make_async_copy(q_hbm.at[pl.ds(0, HALF), :], qin.at[0], load_sem.at[3]),
+        pltpu.make_async_copy(q_hbm, qfull.at[0], load_sem.at[0]),
+        pltpu.make_async_copy(k_hbm, kb.at[0, 0], load_sem.at[1]),
+        pltpu.make_async_copy(v_hbm, vin, load_sem.at[2]),
     ]
     for load in loads:
         load.start()
 
+    lamv[0] = jnp.full((8, HALF), lam_ref[0], f32)
+
     barrier = pltpu.get_barrier_semaphore()
-    for dz, dx in ((0, 1), (0, -1), (1, 0), (-1, 0)):
+    for dz, dx in ((0, 1), (0, -1), (1, 0), (-1, 0), (2, 0), (0, 2)):
         pl.semaphore_signal(barrier, inc=1, device_id=(at(dz, dx), t), device_id_type=MESH)
     for j in range(1, 8):
-        pl.semaphore_signal(barrier, inc=1, device_id=(s, (t + j) % 8), device_id_type=MESH)
-    for j in range(8):
-        pl.semaphore_signal(barrier, inc=1, device_id=(mirror, j), device_id_type=MESH)
-    pl.semaphore_wait(barrier, 19)
-
-    def remote_q():
+        pl.semaphore_signal(barrier, inc=1, device_id=(sp, (t + j) % 8), device_id_type=MESH)
+
+    def along(e, queries, d):
+        own = c if e == 0 else 1 - c
+        first = at(d, 0) if queries else at(0, d)
+        second = at(0, d) if queries else at(d, 0)
+        return jnp.where(own == 0, first, second)
+
+    def piece(kind, slot, part):
+        span = pl.ds(0, BLK) if part == 2 else pl.ds(part * HALF, HALF)
+        if kind == 0:
+            return qfull.at[slot, span, :]
+        if kind == 1:
+            return kb.at[0, slot, span, :]
+        return vb.at[0, slot, :, span]
+
+    def ring_copy(kind, slot, part, lane):
+        d = 1 if lane == 0 else -1
         return pltpu.make_async_remote_copy(
-            src_ref=qin.at[2], dst_ref=qin.at[1], send_sem=qsend, recv_sem=qrecv,
-            device_id=(mirror, t), device_id_type=MESH,
-        )
-
-    def block_copy(which, block, part, lane, device):
-        rows = pl.ds(0, BLK) if part == 2 else pl.ds(part * HALF, HALF)
+            src_ref=piece(kind, slot, part), dst_ref=piece(kind, (slot - d) % 4, part),
+            send_sem=send_sem.at[kind, slot, lane],
+            recv_sem=recv_sem.at[kind, (slot - d) % 4, part % 2],
+            device_id=(along(0, kind == 0, d), t), device_id_type=MESH,
+        )
+
+    RING = ((0, 2, 0), (0, 2, 1), (3, 0, 0), (1, 1, 1))
+
+    def ring_wait(kind, slot):
+        for part in (0, 1) if slot == 2 else (2,):
+            pltpu.make_async_remote_copy(
+                src_ref=piece(kind, slot, part), dst_ref=piece(kind, slot, part),
+                send_sem=send_sem.at[kind, 0, 0], recv_sem=recv_sem.at[kind, slot, part % 2],
+                device_id=(sp, mate), device_id_type=MESH,
+            ).wait_recv()
+
+    def mate_copy(kind, slot):
+        if kind == 0:
+            source = qfull.at[slot, pl.ds(pl.multiple_of((1 - c) * HALF, HALF), HALF), :]
+            target = qother.at[slot]
+        elif kind == 1:
+            source, target = kb.at[0, slot], kb.at[1, slot]
+        else:
+            source, target = vb.at[0, slot], vb.at[1, slot]
         return pltpu.make_async_remote_copy(
-            src_ref=kv.at[which, block, rows, :],
-            dst_ref=kv.at[which, block, rows, :],
-            send_sem=send_sem.at[which, block, lane],
-            recv_sem=recv_sem.at[which, block, part % 2],
-            device_id=(device, t), device_id_type=MESH,
-        )
-
-    lanes = ((0, 1), (0, -1), (1, 0), (-1, 0))
-
-    def sends(which, d):
-        first = which
-        dz, dx = d
-        near, far = (dx, dz) if first == 0 else (dz, dx)
-        near_lanes, far_lanes = ((0, 1), (2, 3)) if first == 0 else ((2, 3), (0, 1))
-        if d == (0, 0):
-            return [(2, near_lanes[0]), (2, near_lanes[1]), (2, far_lanes[0]), (2, far_lanes[1])]
-        if far == 0:
-            out = [(2, far_lanes[0]), (2, far_lanes[1])]
-            if near == -1:
-                out = [(0, near_lanes[0])] + out
-            if near == 1:
-                out = [(1, near_lanes[1])] + out
-            return out
-        if far == -1:
-            return [(0, far_lanes[0])]
-        if far == 1:
-            return [(1, far_lanes[1])]
-        return []
-
-    def halves(which, d):
-        dz, dx = d
-        near, far = (dx, dz) if which == 0 else (dz, dx)
-        return far == 2 or (far == 0 and near == 2)
-
-    def pass_on(which, d):
-        block = at(*d)
-        for part, lane in sends(which, d):
-            block_copy(which, block, part, lane, at(*lanes[lane])).start()
-
-    def arrive(which, d):
-        block = at(*d)
-        for part in (0, 1) if halves(which, d) else (2,):
-            block_copy(which, block, part, 0, s).wait_recv()
-
-    loads[0].wait()
-    remote_q().start()
-    loads[1].wait()
-    loads[2].wait()
-    own_k, own_v = sends(0, (0, 0)), sends(1, (0, 0))
-    for which, part, lane in (
-        [(0,) + own_k[0], (0,) + own_k[1], (1,) + own_v[0], (1,) + own_v[1]]
-        + [(0,) + own_k[2], (0,) + own_k[3], (1,) + own_v[2], (1,) + own_v[3]]
-    ):
-        block_copy(which, s, part, lane, at(*lanes[lane])).start()
-    loads[3].wait()
-
-    mx[...] = jnp.full(mx.shape, -1e30, jnp.float32)
-    acc[...] = jnp.zeros(acc.shape, jnp.float32)
+            src_ref=source, dst_ref=target,
+            send_sem=msend.at[kind, slot], recv_sem=mrecv.at[kind, slot],
+            device_id=(sp, mate), device_id_type=MESH,
+        )
+
+    def lambda_copy():
+        return pltpu.make_async_remote_copy(
+            src_ref=lamv.at[0], dst_ref=lamv.at[1], send_sem=lsend, recv_sem=lrecv,
+            device_id=(sp, mate), device_id_type=MESH,
+        )
+
     lane_ids = lax.broadcasted_iota(jnp.int32, (HALF, 2 * DH), 1)
 
-    def split_maps(half):
-        q = qin[half]
+    def split_maps(e, slot):
+        if e == 0:
+            q = qfull[slot, pl.ds(pl.multiple_of(c * HALF, HALF), HALF), :]
+        else:
+            q = qother[slot]
         zero = jnp.zeros_like(q)
-        qs[half, 0] = jnp.where(lane_ids < DH, q, zero)
-        qs[half, 1] = jnp.where(lane_ids < DH, zero, q)
-
-    split_maps(0)
-    remote_q().wait_recv()
-    split_maps(1)
+        qm[e, slot, 0] = jnp.where(lane_ids < DH, q, zero)
+        qm[e, slot, 1] = jnp.where(lane_ids < DH, zero, q)
+
+    def arrive(kind, slot):
+        ring_wait(kind, slot)
+        if slot == 3:
+            ring_copy(kind, 3, 0, 0).start()
+        if slot == 1:
+            ring_copy(kind, 1, 1, 1).start()
+        mate_copy(kind, slot).start()
+
+    def settle(kind, slot):
+        mate_copy(kind, slot).wait_recv()
+        if kind == 0:
+            split_maps(0, slot)
+            split_maps(1, slot)
+
+    for load in loads:
+        load.wait()
+    pl.semaphore_wait(barrier, 13)
+    for kind in (0, 1):
+        for lane in range(2):
+            ring_copy(kind, 0, 2, lane).start()
+    mate_copy(1, 0).start()
+    mate_copy(0, 0).start()
+    lambda_copy().start()
+    for k in range(4):
+        span = pl.ds(k * 256, 256)
+        vb[0, 0, :, span] = vin[span, :].astype(f32).T.astype(bf16)
+    for lane in range(2):
+        ring_copy(2, 0, 2, lane).start()
+    mate_copy(2, 0).start()
+
+    mx[...] = jnp.full(mx.shape, NEG, f32)
+    acc[...] = jnp.zeros(acc.shape, f32)
 
     scale = LOG2E * DH ** (-0.5)
-    TQ = 256
-
-    def tiles(half, block, masked):
-        k = kv[0, block]
-        v = kv[1, block]
-        ones = jnp.ones_like(v)
-        vv = jnp.concatenate([v, ones], axis=1)
-        for m in range(2):
-            for r in range(HALF // TQ):
-                rows = pl.ds(r * TQ, TQ)
-                scores = lax.dot_general(
-                    qs[half, m, rows, :], k, (((1,), (1,)), ((), ())),
-                    preferred_element_type=jnp.float32,
-                ) * scale
-                if masked:
-                    row_id = lax.broadcasted_iota(jnp.int32, scores.shape, 0) + (half * HALF + r * TQ)
-                    col_id = lax.broadcasted_iota(jnp.int32, scores.shape, 1)
-                    scores = jnp.where(col_id <= row_id, scores, -1e30)
-                old = mx[half, m, rows, :]
-                new = jnp.maximum(old, jnp.max(scores, axis=1, keepdims=True))
-                factor = jnp.exp2(old - new)
-                wide = jnp.concatenate([new] * (BLK // 128), axis=1)
-                weights = jnp.exp2(scores - wide).astype(jnp.bfloat16)
-                pv = jnp.dot(weights, vv, preferred_element_type=jnp.float32)
-                mx[half, m, rows, :] = new
-                acc[half, m, rows, :] = acc[half, m, rows, :] * jnp.concatenate([factor, factor], axis=1) + pv
-
-    def step(i, carry):
-        for k, events in EVENTS.items():
-            @pl.when(i == k)
-            def _(events=events):
-                for kd, vd in events:
-                    arrive(0, kd)
-                    pass_on(0, kd)
-                    arrive(1, vd)
-                    pass_on(1, vd)
-
-        dz = jnp.int32(0)
-        dx = jnp.int32(0)
-        for k, (a, b) in enumerate(ORDER):
-            dz = jnp.where(i == k, a, dz)
-            dx = jnp.where(i == k, b, dx)
-        block = at(dz, dx)
-
-        def one_half(half, c):
-            limit = jnp.where(half == 0, s, mirror)
-
-            @pl.when(block < limit)
+
+    always = sp >= 0
+
+    def tiles(e, di, dk, masked):
+        chunks = [(m, r) for m in range(2) for r in range(HALF // TQ)]
+
+        def phase(now, later):
+            tops, pv = [], None
+            for kk in range(BLK // KB):
+                keys = pl.ds(kk * KB, KB)
+                if later is not None:
+                    m, r = chunks[later]
+                    scores = lax.dot_general(
+                        kb[e, dk, keys, :], qm[e, di, m, pl.ds(r * TQ, TQ), :],
+                        (((1,), (1,)), ((), ())), preferred_element_type=f32,
+                    ) * scale
+                    if masked:
+                        key_id = lax.broadcasted_iota(jnp.int32, scores.shape, 0) + kk * KB
+                        query_id = lax.broadcasted_iota(jnp.int32, scores.shape, 1) + (c * HALF + r * TQ)
+                        scores = jnp.where(key_id <= query_id, scores, NEG)
+                    sbuf[later % 2][keys, :] = scores
+                    tops.append(jnp.max(scores, axis=0, keepdims=True))
+                if now is not None:
+                    m, r = chunks[now]
+                    values = jnp.concatenate(
+                        [vb[e, dk, :, keys], jnp.ones((VROWS - 128, KB), bf16)], axis=0
+                    )
+                    weights = jnp.exp2(sbuf[now % 2][keys, :] - nbuf[now % 2][...]).astype(bf16)
+                    term = jnp.dot(values, weights, preferred_element_type=f32)
+                    pv = term if pv is None else pv + term
+            if now is not None:
+                m, r = chunks[now]
+                cols = pl.ds(r * TQ, TQ)
+                acc[e, di, m, :, cols] = acc[e, di, m, :, cols] * fbuf[now % 2][...] + pv
+            if later is not None:
+                m, r = chunks[later]
+                cols = pl.ds(r * TQ, TQ)
+                old = mx[e, di, m, :, cols]
+                new = functools.reduce(jnp.maximum, tops, old)
+                fbuf[later % 2][...] = jnp.exp2(old - new)
+                nbuf[later % 2][...] = new
+                mx[e, di, m, :, cols] = new
+
+        phase(None, 0)
+        for n in range(len(chunks)):
+            @pl.when(always)
+            def _(n=n):
+                phase(n, n + 1 if n + 1 < len(chunks) else None)
+
+    def partial_copies(e, d):
+        to = along(e, True, d)
+        slot = (4 - d) % 4
+        return [
+            pltpu.make_async_remote_copy(
+                src_ref=pout.at[e, d], dst_ref=pin.at[e, slot],
+                send_sem=psend.at[e, d], recv_sem=precv.at[e, slot],
+                device_id=(to, t), device_id_type=MESH,
+            ),
+            pltpu.make_async_remote_copy(
+                src_ref=sout.at[e, d], dst_ref=sin.at[e, slot],
+                send_sem=ssend.at[e, d], recv_sem=srecv.at[e, slot],
+                device_id=(to, t), device_id_type=MESH,
+            ),
+        ]
+
+    def normal(e, d, m):
+        total = acc[e, d, m, pl.ds(128, 1), :]
+        some = total > 0.0
+        safe = jnp.where(some, total, 1.0)
+        level = jnp.where(some, mx[e, d, m] + jnp.log2(safe), NEG)
+        return acc[e, d, m, pl.ds(0, 128), :] / safe, level
+
+    def send_partial(d):
+        for e in range(2):
+            for m in range(2):
+                value, level = normal(e, d, m)
+                pout[e, d, m] = value.astype(bf16)
+                sout[e, d, m] = jnp.broadcast_to(level, (8, HALF))
+            for copy in partial_copies(e, d):
+                copy.start()
+
+    def before(n):
+        if n == 0:
+            for kind in (1, 0, 2):
+                settle(kind, 0)
+        if n == 1:
+            for kind in range(3):
+                for slot in (3, 1):
+                    arrive(kind, slot)
+            for kind in range(3):
+                for slot in (3, 1):
+                    settle(kind, slot)
+        if n == 4:
+            for kind in range(3):
+                arrive(kind, 2)
+            for kind in range(3):
+                settle(kind, 2)
+        if n == 11:
+            send_partial(2)
+        if n == 12:
+            send_partial(3)
+        if n == 13:
+            send_partial(1)
+
+    def step(n, carry):
+        for k in (0, 1, 4, 11, 12, 13):
+            @pl.when(n == k)
+            def _(k=k):
+                before(k)
+
+        di = jnp.int32(0)
+        dk = jnp.int32(0)
+        for k, (a, b) in enumerate(WORK):
+            di = jnp.where(n == k, a, di)
+            dk = jnp.where(n == k, b, dk)
+
+        def one_head(e, inner):
+            head = jnp.where(e == 0, c, 1 - c)
+            query_block = jnp.where(head == 0, at(di, 0), at(0, di))
+            key_block = jnp.where(head == 0, at(0, dk), at(dk, 0))
+
+            @pl.when(key_block < query_block)
             def _():
-                tiles(half, block, False)
-
-            @pl.when(block == limit)
+                tiles(e, di, dk, False)
+
+            @pl.when(key_block == query_block)
             def _():
-                tiles(half, block, True)
-
-            return c
-
-        return lax.fori_loop(0, 2, one_half, carry)
-
-    lax.fori_loop(0, NZ * NX, step, 0)
-
-    lam = lam_ref[0]
-    gain = gain_ref[...]
-    for half in range(2):
-        for r in range(HALF // 128):
-            rows = pl.ds(r * 128, 128)
-            mixed = [acc[half, m, rows, :128] / acc[half, m, rows, 128:] for m in range(2)]
-            contrast = mixed[0] - lam * mixed[1]
-            mean = jnp.mean(contrast * contrast, axis=1, keepdims=True)
-            obuf[half, rows, :] = (contrast * lax.rsqrt(mean + 1e-05) * gain).astype(jnp.bfloat16)
-    columns = pl.ds(pl.multiple_of(t * 128, 128), 128)
-
-    def out_copy(half, j, sender):
-        rows = pl.ds(j * 128, 128)
+                tiles(e, di, dk, True)
+
+            return inner
+
+        return lax.fori_loop(0, 2, one_head, carry)
+
+    lax.fori_loop(0, len(WORK), step, 0)
+
+    def out_copy(e, j, sender):
         cols = pl.ds(pl.multiple_of(sender * 128, 128), 128)
         return pltpu.make_async_remote_copy(
-            src_ref=obuf.at[half, rows, :], dst_ref=out_ref.at[:, cols],
-            send_sem=osend.at[half, j], recv_sem=orecv.at[sender],
-            device_id=(s if half == 0 else mirror, 4 * half + j), device_id_type=MESH,
-        )
-
-    for j in range(4):
-        out_copy(1, j, t).start()
-        @pl.when(t != j)
-        def _():
-            out_copy(0, j, t).start()
-        @pl.when(t == j)
-        def _():
-            out_ref[:, columns] = obuf[0, j * 128:(j + 1) * 128, :]
-    for j in range(8):
-        @pl.when(jnp.logical_or(t >= 4, t != j))
-        def _():
-            out_copy(0, 0, j).wait_recv()
-    for j in range(4):
-        out_copy(1, j, t).wait_send()
-        @pl.when(t != j)
-        def _():
-            out_copy(0, j, t).wait_send()
-    remote_q().wait_send()
-    for which in range(2):
-        for d in ORDER:
-            for part, lane in sends(which, d):
-                block_copy(which, at(*d), part, lane, s).wait_send()
+            src_ref=obuf.at[e, pl.ds(j * 128, 128), :], dst_ref=out_ref.at[:, cols],
+            send_sem=osend.at[e, j], recv_sem=orecv.at[sender],
+            device_id=(sp, 4 * c + j), device_id_type=MESH,
+        )
+
+    lambda_copy().wait_recv()
+    for e in range(2):
+        head = t if e == 0 else mate
+        for slot in (2, 1, 3):
+            pltpu.make_async_remote_copy(
+                src_ref=pout.at[e, slot], dst_ref=pin.at[e, slot],
+                send_sem=psend.at[e, slot], recv_sem=precv.at[e, slot],
+                device_id=(sp, mate), device_id_type=MESH,
+            ).wait_recv()
+            pltpu.make_async_remote_copy(
+                src_ref=sout.at[e, slot], dst_ref=sin.at[e, slot],
+                send_sem=ssend.at[e, slot], recv_sem=srecv.at[e, slot],
+                device_id=(sp, mate), device_id_type=MESH,
+            ).wait_recv()
+        mixed = []
+        for m in range(2):
+            value, level = normal(e, 0, m)
+            levels = [level] + [sin[e, slot, m, pl.ds(0, 1), :] for slot in (1, 2, 3)]
+            top = jnp.maximum(jnp.maximum(levels[0], levels[1]), jnp.maximum(levels[2], levels[3]))
+            share = [jnp.exp2(item - top) for item in levels]
+            inverse = 1.0 / (share[0] + share[1] + share[2] + share[3])
+            total = value * (share[0] * inverse)
+            for slot in (1, 2, 3):
+                total = total + pin[e, slot, m].astype(f32) * (share[slot] * inverse)
+            mixed.append(total)
+        contrast = mixed[0] - lamv[e, pl.ds(0, 1), :] * mixed[1]
+        mean = jnp.mean(contrast * contrast, axis=0, keepdims=True)
+        contrast = contrast * lax.rsqrt(mean + 1e-05)
+        for j in range(4):
+            rows = contrast[:, j * 128:(j + 1) * 128].T * gain_ref[...]
+            obuf[e, pl.ds(j * 128, 128), :] = rows.astype(bf16)
+        for j in range(4):
+            @pl.when(t != 4 * c + j)
+            def _(e=e, j=j, head=head):
+                out_copy(e, j, head).start()
+            @pl.when(t == 4 * c + j)
+            def _(e=e, j=j, head=head):
+                cols = pl.ds(pl.multiple_of(head * 128, 128), 128)
+                out_ref[:, cols] = obuf[e, pl.ds(j * 128, 128), :]
+
+    origin = t // 4
+    for yy in range(4):
+        for core in range(2):
+            @pl.when(2 * yy + origin != t)
+            def _(yy=yy, core=core):
+                out_copy(0, 0, 2 * yy + core).wait_recv()
+    for e in range(2):
+        for j in range(4):
+            @pl.when(t != 4 * c + j)
+            def _(e=e, j=j):
+                out_copy(e, j, t).wait_send()
+    lambda_copy().wait_send()
+    for kind in range(3):
+        for slot, part, lane in RING:
+            ring_copy(kind, slot, part, lane).wait_send()
+        for slot in range(4):
+            mate_copy(kind, slot).wait_send()
+    for e in range(2):
+        for d in (1, 2, 3):
+            for copy in partial_copies(e, d):
+                copy.wait_send()
 
 
 def attention(lambdas, head_gain, queries, key_rows, value_rows):
     any_space = pl.BlockSpec(memory_space=pl.ANY)
+    bf16, f32 = jnp.bfloat16, jnp.float32
+    dma = pltpu.SemaphoreType.DMA
     return pl.pallas_call(
         attention_kernel,
         out_shape=jax.ShapeDtypeStruct((128, 1024), jnp.bfloat16),
@@ -259,19 +376,30 @@
         ],
         out_specs=pl.BlockSpec(memory_space=pltpu.VMEM),
         scratch_shapes=[
-            pltpu.VMEM((2, NZ * NX, BLK, 128), jnp.bfloat16),
-            pltpu.VMEM((3, HALF, 128), jnp.bfloat16),
-            pltpu.VMEM((2, 2, HALF, 128), jnp.bfloat16),
-            pltpu.VMEM((2, 2, HALF, 128), jnp.float32),
-            pltpu.VMEM((2, 2, HALF, 256), jnp.float32),
-            pltpu.VMEM((2, HALF, 128), jnp.bfloat16),
-            pltpu.SemaphoreType.DMA((4,)),
-            pltpu.SemaphoreType.DMA,
-            pltpu.SemaphoreType.DMA,
-            pltpu.SemaphoreType.DMA((2, NZ * NX, 4)),
-            pltpu.SemaphoreType.DMA((2, NZ * NX, 2)),
-            pltpu.SemaphoreType.DMA((2, 4)),
-            pltpu.SemaphoreType.DMA((8,)),
+            pltpu.VMEM((BLK, 128), bf16),
+            pltpu.VMEM((2, 8, HALF), f32),
+            pltpu.VMEM((4, BLK, 128), bf16),
+            pltpu.VMEM((4, HALF, 128), bf16),
+            pltpu.VMEM((2, 4, BLK, 128), bf16),
+            pltpu.VMEM((2, 4, 128, BLK), bf16),
+            pltpu.VMEM((2, 4, 2, HALF, 128), bf16),
+            pltpu.VMEM((2, 4, 2, 1, HALF), f32),
+            pltpu.VMEM((2, 4, 2, VROWS, HALF), f32),
+            pltpu.VMEM((2, 4, 2, 128, HALF), bf16),
+            pltpu.VMEM((2, 4, 2, 128, HALF), bf16),
+            pltpu.VMEM((2, 4, 2, 8, HALF), f32),
+            pltpu.VMEM((2, 4, 2, 8, HALF), f32),
+            pltpu.VMEM((2, HALF, 128), bf16),
+            pltpu.VMEM((BLK, TQ), f32), pltpu.VMEM((BLK, TQ), f32),
+            pltpu.VMEM((1, TQ), f32), pltpu.VMEM((1, TQ), f32),
+            pltpu.VMEM((1, TQ), f32), pltpu.VMEM((1, TQ), f32),
+            dma((3,)),
+            dma, dma,
+            dma((3, 4, 2)), dma((3, 4, 2)),
+            dma((3, 4)), dma((3, 4)),
+            dma((2, 4)), dma((2, 4)),
+            dma((2, 4)), dma((2, 4)),
+            dma((2, 4)), dma((8,)),
         ],
         compiler_params=pltpu.CompilerParams(
             collective_id=0, has_side_effects=True, vmem_limit_bytes=48 * 1024 * 1024

time: 206 us -> 191 us (0.927)
  Pallas kernels: 196 us -> 181 us
    pallas_call x1, Pallas kernels: 124 us -> 115 us  [routed_experts(): pl.pallas_call(expert_kernel, out_shape=jax.ShapeDtypeStruct((128, WID),...]
    pallas_call x1, Pallas kernels: 72.2 us -> 65.4 us  [attention(): pl.pallas_call(attention_kernel, out_shape=jax.ShapeDtypeStruct((128, 102...]
where the time goes in v3:
time: 191 us; the launch traced here: 190 us
  Pallas kernels  181 us (95%)
  local copies, waits for them, and re-layouts  8.9 us (5%)
    pallas_call x1, Pallas kernels, routed_experts(): pl.pallas_call(expert_kernel, out_shape=jax.ShapeDtypeStruct((128, WID),...  115 us
    pallas_call x1, Pallas kernels, attention(): pl.pallas_call(attention_kernel, out_shape=jax.ShapeDtypeStruct((128, 102...  65.4 us
    unnamed x13, local copies, waits for them, and re-layouts  8.9 us

profile of v3, /device:TPU:1, one launch (start us, length us, event | category | flops | bytes accessed | tf_op | source)
XLA Modules:
  0.0 190.2 jit_solution(5710335367081234218)
XLA Ops:
  0.7 1.4 copy.14.routes_ref
  2.1 1.4 copy.15.rw_ref
  3.5 0.0 copy-start.1
  3.5 0.9 copy-done.1
  4.4 0.0 copy-start.2
  4.4 0.9 copy-done.2
  5.4 0.0 copy-start.3
  5.4 0.9 copy-done.3
  6.3 0.0 copy-start.4
  6.3 0.7 copy-done.4
  7.0 65.4 %attention.1.heads_ref = bf16[128,1024]{1,0:T(8,128)(2,1)S(1)} custom-call(f32[1]{0:T(128)S(6)} %copy.17.lam_ref, f32[1,128]{1,0:T(1,128)S(1)} %bitcast.2, bf16[1024,128]{1,0:T(8,128)(2,1)S(1)} %copy-done.1, bf16[1024,128]{1,0:T(8,128)(2,1)S(1)} %copy-done.2, bf16[1024,128]{1,0:T(8,128)(2,1)S(1)} %copy-done.3), custom_call_target="tpu_custom_call" | custom-call | tf_op jit(solution)/shard_map/attention/pallas_call | solution.py:369
  72.3 0.0 copy-start
  72.3 0.7 copy-done
  73.0 115.3 %experts.1 = bf16[128,2048]{1,0:T(8,128)(2,1)} custom-call(bf16[128,1024]{1,0:T(8,128)(2,1)} %copy-done, bf16[128,2048]{1,0:T(8,128)(2,1)} %stream_ref.1, f32[1,2048]{1,0:T(1,128)} %bitcast.3, s32[128,2]{1,0:T(8,128)} %copy.14.routes_ref, f32[128,2]{1,0:T(8,128)} %copy.15.rw_ref, bf16[1024,2048]{1,0:T(8,128)(2,1)} %ow_hbm.1, bf16[1,2048,640]{2,1,0:T(8,128)(2,1)} %gate_hbm.1, ...), custom_call_target="tpu_custom_call" | custom-call | tf_op jit(solution)/shard_map/experts/pallas_call | solution.py:726
  188.3 1.9 copy.18
Async XLA Ops:
  3.5 0.9 copy-start.1
  4.4 0.9 copy-start.2
  5.4 0.9 copy-start.3
  6.3 0.7 copy-start.4
  72.3 0.7 copy-start

commit v4 on v3

--- a/solution.py
+++ b/solution.py
@@ -21,14 +21,14 @@
 TQ = 512
 KB = 256
 WORK = (
-    (0, 0), (3, 0), (1, 0), (3, 3), (1, 3), (3, 1), (1, 1),
-    (2, 0), (2, 3), (2, 1), (2, 2), (3, 2), (1, 2), (0, 3), (0, 1), (0, 2),
+    (0, 0), (3, 0), (1, 0), (3, 3), (3, 1), (1, 3), (1, 1), (3, 2), (1, 2),
+    (2, 0), (2, 3), (2, 1), (2, 2), (0, 3), (0, 1), (0, 2),
 )
 
 
 def attention_kernel(
-    lam_ref, gain_ref, q_hbm, k_hbm, v_hbm, out_ref,
-    vin, lamv, qfull, qother, kb, vb, qm, mx, acc, pout, pin, sout, sin, obuf, sbuf0, sbuf1, fbuf0, fbuf1, nbuf0, nbuf1,
+    lam_hbm, gain_hbm, q_hbm, k_hbm, v_hbm, out_ref,
+    lam_ref, gain_ref, vin, lamv, qfull, qother, kb, vb, qm, mx, acc, pout, pin, sout, sin, obuf, sbuf0, sbuf1, fbuf0, fbuf1, nbuf0, nbuf1,
     load_sem, lsend, lrecv, send_sem, recv_sem, msend, mrecv, psend, precv, ssend, srecv, osend, orecv,
 ):
     sp = lax.axis_index("sp")
@@ -47,10 +47,12 @@
         pltpu.make_async_copy(k_hbm, kb.at[0, 0], load_sem.at[1]),
         pltpu.make_async_copy(v_hbm, vin, load_sem.at[2]),
     ]
-    for load in loads:
+    small = [
+        pltpu.make_async_copy(lam_hbm, lam_ref, load_sem.at[3]),
+        pltpu.make_async_copy(gain_hbm, gain_ref, load_sem.at[4]),
+    ]
+    for load in loads + small:
         load.start()
-
-    lamv[0] = jnp.full((8, HALF), lam_ref[0], f32)
 
     barrier = pltpu.get_barrier_semaphore()
     for dz, dx in ((0, 1), (0, -1), (1, 0), (-1, 0), (2, 0), (0, 2)):
@@ -136,8 +138,9 @@
             split_maps(0, slot)
             split_maps(1, slot)
 
-    for load in loads:
+    for load in loads + small:
         load.wait()
+    lamv[0] = jnp.full((8, HALF), lam_ref[0], f32)
     pl.semaphore_wait(barrier, 13)
     for kind in (0, 1):
         for lane in range(2):
@@ -248,20 +251,20 @@
             for kind in range(3):
                 for slot in (3, 1):
                     settle(kind, slot)
-        if n == 4:
+        if n == 5:
             for kind in range(3):
                 arrive(kind, 2)
             for kind in range(3):
                 settle(kind, 2)
-        if n == 11:
+        if n == 8:
+            send_partial(3)
+        if n == 9:
+            send_partial(1)
+        if n == 13:
             send_partial(2)
-        if n == 12:
-            send_partial(3)
-        if n == 13:
-            send_partial(1)
 
     def step(n, carry):
-        for k in (0, 1, 4, 11, 12, 13):
+        for k in (0, 1, 5, 8, 9, 13):
             @pl.when(n == k)
             def _(k=k):
                 before(k)
@@ -299,10 +302,16 @@
             device_id=(sp, 4 * c + j), device_id_type=MESH,
         )
 
+    def own_copy(e, j, head):
+        cols = pl.ds(pl.multiple_of(head * 128, 128), 128)
+        return pltpu.make_async_copy(
+            obuf.at[e, pl.ds(j * 128, 128), :], out_ref.at[:, cols], osend.at[e, j]
+        )
+
     lambda_copy().wait_recv()
     for e in range(2):
         head = t if e == 0 else mate
-        for slot in (2, 1, 3):
+        for slot in (1, 3, 2):
             pltpu.make_async_remote_copy(
                 src_ref=pout.at[e, slot], dst_ref=pin.at[e, slot],
                 send_sem=psend.at[e, slot], recv_sem=precv.at[e, slot],
@@ -336,8 +345,7 @@
                 out_copy(e, j, head).start()
             @pl.when(t == 4 * c + j)
             def _(e=e, j=j, head=head):
-                cols = pl.ds(pl.multiple_of(head * 128, 128), 128)
-                out_ref[:, cols] = obuf[e, pl.ds(j * 128, 128), :]
+                own_copy(e, j, head).start()
 
     origin = t // 4
     for yy in range(4):
@@ -350,6 +358,9 @@
             @pl.when(t != 4 * c + j)
             def _(e=e, j=j):
                 out_copy(e, j, t).wait_send()
+            @pl.when(t == 4 * c + j)
+            def _(e=e, j=j):
+                own_copy(e, j, t).wait()
     lambda_copy().wait_send()
     for kind in range(3):
         for slot, part, lane in RING:
@@ -363,19 +374,19 @@
 
 
 def attention(lambdas, head_gain, queries, key_rows, value_rows):
-    any_space = pl.BlockSpec(memory_space=pl.ANY)
+    any_space = pl.BlockSpec(memory_space=pltpu.HBM)
     bf16, f32 = jnp.bfloat16, jnp.float32
     dma = pltpu.SemaphoreType.DMA
     return pl.pallas_call(
         attention_kernel,
         out_shape=jax.ShapeDtypeStruct((128, 1024), jnp.bfloat16),
         in_specs=[
-            pl.BlockSpec(memory_space=pltpu.SMEM),
-            pl.BlockSpec(memory_space=pltpu.VMEM),
-            any_space, any_space, any_space,
+            any_space, any_space, any_space, any_space, any_space,
         ],
-        out_specs=pl.BlockSpec(memory_space=pltpu.VMEM),
+        out_specs=any_space,
         scratch_shapes=[
+            pltpu.SMEM((1,), f32),
+            pltpu.VMEM((1, 128), f32),
             pltpu.VMEM((BLK, 128), bf16),
             pltpu.VMEM((2, 8, HALF), f32),
             pltpu.VMEM((4, BLK, 128), bf16),
@@ -393,7 +404,7 @@
             pltpu.VMEM((BLK, TQ), f32), pltpu.VMEM((BLK, TQ), f32),
             pltpu.VMEM((1, TQ), f32), pltpu.VMEM((1, TQ), f32),
             pltpu.VMEM((1, TQ), f32), pltpu.VMEM((1, TQ), f32),
-            dma((3,)),
+            dma((5,)),
             dma, dma,
             dma((3, 4, 2)), dma((3, 4, 2)),
             dma((3, 4)), dma((3, 4)),
@@ -402,7 +413,7 @@
             dma((2, 4)), dma((8,)),
         ],
         compiler_params=pltpu.CompilerParams(
-            collective_id=0, has_side_effects=True, vmem_limit_bytes=48 * 1024 * 1024
+            collective_id=0, has_side_effects=True, vmem_limit_bytes=67043328
         ),
         name="attention",
     )(lambdas, head_gain.reshape(1, -1), queries, key_rows, value_rows)
@@ -419,9 +430,9 @@
 
 
 def expert_kernel(
-    heads_ref, stream_ref, gain_ref, routes_ref, rw_ref, ow_hbm, gate_hbm, up_hbm, down_hbm,
+    heads_hbm, stream_hbm, gain_hbm, routes_hbm, rw_hbm, ow_hbm, gate_hbm, up_hbm, down_hbm,
     out_ref,
-    ow, gw, uw, dw, att, nrm, outg, arr, reto, ret, xs, act, ps, pr, rh, rf, cm, cr,
+    heads_ref, stream_ref, gain_ref, routes_ref, rw_ref, ow, gw, uw, dw, att, nrm, outg, arr, reto, ret, xs, act, ps, pr, rh, rf, cm, cr,
     load_sem, psend, precv, xsend, xrecv, qsend, qrecv, rsend, rhrecv, rfrecv, bsend, brecv,
 ):
     s = lax.axis_index("sp")
@@ -443,7 +454,14 @@
         pltpu.make_async_copy(up_hbm.at[0], uw, load_sem.at[2]),
         pltpu.make_async_copy(down_hbm.at[0], dw, load_sem.at[3]),
     ]
-    for load in loads:
+    small = [
+        pltpu.make_async_copy(routes_hbm, routes_ref, load_sem.at[4]),
+        pltpu.make_async_copy(rw_hbm, rw_ref, load_sem.at[5]),
+        pltpu.make_async_copy(stream_hbm, stream_ref, load_sem.at[6]),
+        pltpu.make_async_copy(gain_hbm, gain_ref, load_sem.at[7]),
+        pltpu.make_async_copy(heads_hbm, heads_ref, load_sem.at[8]),
+    ]
+    for load in small + loads:
         load.start()
 
     barrier = pltpu.get_barrier_semaphore()
@@ -453,7 +471,8 @@
     for peer in (lane(1, c), lane(-1, c), mate):
         pl.semaphore_signal(barrier, inc=1, device_id=(s, peer), device_id_type=MESH)
 
-    loads[0].wait()
+    for load in small + loads[:1]:
+        load.wait()
     heads = heads_ref[...]
     square = jnp.zeros((128, 1), f32)
     for k in range(0, WID, 512):
@@ -466,43 +485,41 @@
         cols = pl.ds(k, 512)
         nrm[:, cols] = (att[:, cols] * inverse * gain_ref[:, cols]).astype(bf16)
 
-    experts = lax.broadcasted_iota(jnp.int32, (128, 16), 1)
-    route = [routes_ref[:, k:k + 1] for k in range(2)]
+    experts = lax.broadcasted_iota(jnp.int32, (16, 128), 0)
+    route = [routes_ref[pl.ds(k, 1), :] for k in range(2)]
     hot = [(r == experts).astype(f32) for r in route]
     row_id = lax.broadcasted_iota(jnp.int32, (128, 128), 0)
     col_id = lax.broadcasted_iota(jnp.int32, (128, 128), 1)
-    earlier = (col_id < row_id).astype(f32).astype(bf16)
-    before = jnp.dot(earlier, (hot[0] + hot[1]).astype(bf16), preferred_element_type=f32)
-    place = lax.broadcasted_iota(jnp.int32, (128, 256), 1).astype(f32)
+    earlier = (row_id < col_id).astype(f32).astype(bf16)
+    before = jnp.dot((hot[0] + hot[1]).astype(bf16), earlier, preferred_element_type=f32)
+    place = lax.broadcasted_iota(jnp.int32, (256, 128), 0).astype(f32)
     main_hit, rem_hit = [], []
     for k in range(2):
-        slot = jnp.sum(before * hot[k], axis=1, keepdims=True)
+        slot = jnp.sum(before * hot[k], axis=0, keepdims=True)
         base = route[k].astype(f32) * 16.0 + slot
         low = slot < float(MAIN)
         main_hit.append((jnp.where(low, base, -1.0) == place).astype(f32))
         rem_hit.append([
             (jnp.where(low, -1.0, base + (4.0 * j - 16.0)) == place).astype(f32) for j in range(4)
         ])
-    weight = [rw_ref[:, k:k + 1] for k in range(2)]
+    weight = [rw_ref[pl.ds(k, 1), :] for k in range(2)]
     over_rows = (((0,), (0,)), ((), ()))
     chosen = (main_hit[0] + main_hit[1]).astype(bf16)
     for k in range(0, WID, 512):
         cols = pl.ds(k, 512)
-        outg[:, cols] = lax.dot_general(
-            chosen, nrm[:, cols], over_rows, preferred_element_type=f32
-        ).astype(bf16)
+        outg[:, cols] = jnp.dot(chosen, nrm[:, cols], preferred_element_type=f32).astype(bf16)
     extra = jnp.zeros((256, REM), f32)
     for j in range(4):
-        extra = extra + lax.dot_general(
-            (rem_hit[0][j] + rem_hit[1][j]).astype(bf16), nrm[:, pl.ds(j * REM, REM)], over_rows,
+        extra = extra + jnp.dot(
+            (rem_hit[0][j] + rem_hit[1][j]).astype(bf16), nrm[:, pl.ds(j * REM, REM)],
             preferred_element_type=f32,
         )
     outg[:, pl.ds(WID, REM)] = extra.astype(bf16)
 
     def keep_split(ref, value):
         high = value.astype(bf16)
-        ref[:, pl.ds(0, 256)] = high
-        ref[:, pl.ds(256, 256)] = (value - high.astype(f32)).astype(bf16)
+        ref[pl.ds(0, 256), :] = high
+        ref[pl.ds(256, 256), :] = (value - high.astype(f32)).astype(bf16)
 
     pl.semaphore_wait(barrier, len(others) + 3)
 
@@ -698,9 +715,10 @@
         cols = pl.ds(j * REM, REM)
         back = ret[:, cols]
         tail = ret[:, pl.ds(WID, REM)]
-        routed = jnp.dot(cm[...], jnp.concatenate([back, back], axis=0), preferred_element_type=f32)
-        routed = routed + jnp.dot(
-            cr[j], jnp.concatenate([tail, tail], axis=0), preferred_element_type=f32
+        routed = lax.dot_general(
+            cm[...], jnp.concatenate([back, back], axis=0), over_rows, preferred_element_type=f32
+        ) + lax.dot_general(
+            cr[j], jnp.concatenate([tail, tail], axis=0), over_rows, preferred_element_type=f32
         )
         out_ref[:, cols] = (att[:, cols] + routed).astype(bf16)
 
@@ -719,16 +737,21 @@
 def routed_experts(
     heads, stream, ffn_gain, routes, route_weight, out_weight, gate_weight, up_weight, down_weight
 ):
-    any_space = pl.BlockSpec(memory_space=pl.ANY)
+    any_space = pl.BlockSpec(memory_space=pltpu.HBM)
     vmem = pl.BlockSpec(memory_space=pltpu.VMEM)
     bf16, f32 = jnp.bfloat16, jnp.float32
     dma = pltpu.SemaphoreType.DMA
     return pl.pallas_call(
         expert_kernel,
         out_shape=jax.ShapeDtypeStruct((128, WID), bf16),
-        in_specs=[vmem] * 5 + [any_space] * 4,
+        in_specs=[any_space] * 9,
         out_specs=vmem,
         scratch_shapes=[
+            pltpu.VMEM((128, 1024), bf16),
+            pltpu.VMEM((128, WID), bf16),
+            pltpu.VMEM((1, WID), f32),
+            pltpu.VMEM((2, 128), jnp.int32),
+            pltpu.VMEM((2, 128), f32),
             pltpu.VMEM((1024, WID), bf16),
             pltpu.VMEM((WID, 640), bf16),
             pltpu.VMEM((WID, 640), bf16),
@@ -745,9 +768,9 @@
             pltpu.VMEM((4, 4, CH, WID), bf16),
             pltpu.VMEM((4, 2, CH, HW), bf16),
             pltpu.VMEM((4, 2, 2, CH, HW), bf16),
-            pltpu.VMEM((128, 512), bf16),
-            pltpu.VMEM((4, 128, 512), bf16),
-            dma((4,)),
+            pltpu.VMEM((512, 128), bf16),
+            pltpu.VMEM((4, 512, 128), bf16),
+            dma((9,)),
             dma((16,)), dma((16,)),
             dma((4, 8)), dma((4, 8, 2)),
             dma((4, 4)), dma((4, 4)),
@@ -755,11 +778,11 @@
             dma((16,)), dma((16,)),
         ],
         compiler_params=pltpu.CompilerParams(
-            collective_id=1, has_side_effects=True, vmem_limit_bytes=63 * 1024 * 1024
+            collective_id=1, has_side_effects=True, vmem_limit_bytes=67043328
         ),
         name="experts",
     )(
-        heads, stream, ffn_gain.reshape(1, -1), routes, route_weight,
+        heads, stream, ffn_gain.reshape(1, -1), routes.T, route_weight.T,
         out_weight, gate_weight, up_weight, down_weight,
     )
 

time: 191 us -> 179 us (0.937)
  local copies, waits for them, and re-layouts: 8.9 us -> 1.88 us
  Pallas kernels: 181 us -> 177 us
    unnamed x13 -> x1, local copies, waits for them, and re-layouts: 8.9 us -> 1.88 us
    pallas_call x1, Pallas kernels: 65.4 us -> 61.4 us  [attention(): pl.pallas_call(attention_kernel, out_shape=jax.ShapeDtypeStruct((128, 102...]
where the time goes in v4:
time: 179 us
  Pallas kernels  177 us (99%)
  local copies, waits for them, and re-layouts  1.88 us (1%)
    pallas_call x1, Pallas kernels, routed_experts(): pl.pallas_call(expert_kernel, out_shape=jax.ShapeDtypeStruct((128, WID),...  115 us
    pallas_call x1, Pallas kernels, attention(): pl.pallas_call(attention_kernel, out_shape=jax.ShapeDtypeStruct((128, 102...  61.4 us

profile of v4, /device:TPU:1, one launch (start us, length us, event | category | flops | bytes accessed | tf_op | source)
XLA Modules:
  0.0 179.1 jit_solution(16009797602796133943)
XLA Ops:
  0.7 61.4 %attention.1.heads_hbm = bf16[128,1024]{1,0:T(8,128)(2,1)} custom-call(f32[1]{0:T(128)S(6)} %copy.15.lam_hbm, f32[1,128]{1,0:T(1,128)} %bitcast.7, bf16[1024,128]{1,0:T(8,128)(2,1)} %q_hbm.1, bf16[1024,128]{1,0:T(8,128)(2,1)} %k_hbm.1, bf16[1024,128]{1,0:T(8,128)(2,1)} %v_hbm.1), custom_call_target="tpu_custom_call" | custom-call | tf_op jit(solution)/shard_map/attention/pallas_call | solution.py:380
  62.1 115.1 %experts.1 = bf16[128,2048]{1,0:T(8,128)(2,1)} custom-call(bf16[128,1024]{1,0:T(8,128)(2,1)} %attention.1.heads_hbm, bf16[128,2048]{1,0:T(8,128)(2,1)} %stream_hbm.1, f32[1,2048]{1,0:T(1,128)} %bitcast.4, s32[2,128]{1,0:T(2,128)} %bitcast.5, f32[2,128]{1,0:T(2,128)} %bitcast.6, bf16[1024,2048]{1,0:T(8,128)(2,1)} %ow_hbm.1, bf16[1,2048,640]{2,1,0:T(8,128)(2,1)} %gate_hbm.1, ...), custom_call_target="tpu_custom_call" | custom-call | tf_op jit(solution)/shard_map/experts/pallas_call | solution.py:744
  177.2 1.9 %copy.16 = bf16[128,2048]{1,0:T(8,128)(2,1)} copy(bf16[128,2048]{1,0:T(8,128)(2,1)} %experts.1) | data formatting | bytes 1048576

commit v5 on v4

--- a/solution.py
+++ b/solution.py
@@ -424,6 +424,9 @@
 CH = 80
 WID = 2048
 HW = 1024
+AW = 1024
+AH = AW // 2
+REMA = AW // 4
 REM = 512
 BAND = WID + REM
 NT = 8
@@ -432,8 +435,8 @@
 def expert_kernel(
     heads_hbm, stream_hbm, gain_hbm, routes_hbm, rw_hbm, ow_hbm, gate_hbm, up_hbm, down_hbm,
     out_ref,
-    heads_ref, stream_ref, gain_ref, routes_ref, rw_ref, ow, gw, uw, dw, att, nrm, outg, arr, reto, ret, xs, act, ps, pr, rh, rf, cm, cr,
-    load_sem, psend, precv, xsend, xrecv, qsend, qrecv, rsend, rhrecv, rfrecv, bsend, brecv,
+    heads_ref, stream_ref, gain_ref, routes_ref, rw_ref, infos, toks, outb, arrb, ow, gw, uw, dw, att, nrm, outg, arr, reto, ret, xs, act, ps, pr, rh, rf, cm, cr,
+    load_sem, isend, irecv, tsend, trecv, obsend, obrecv, xbsend, xbrecv, psend, precv, xsend, xrecv, qsend, qrecv, rsend, rhrecv, rfrecv, bsend, brecv,
 ):
     s = lax.axis_index("sp")
     t = lax.axis_index("tp")
@@ -468,7 +471,7 @@
     others = [(dz, dx) for dz in GROUPS for dx in (0, 1, -1, 2) if (dz, dx) != (0, 0)]
     for dz, dx in others:
         pl.semaphore_signal(barrier, inc=1, device_id=(at(dz, dx), t), device_id_type=MESH)
-    for peer in (lane(1, c), lane(-1, c), mate):
+    for peer in (lane(1, c), lane(-1, c), lane(2, c), mate):
         pl.semaphore_signal(barrier, inc=1, device_id=(s, peer), device_id_type=MESH)
 
     for load in small + loads[:1]:
@@ -483,45 +486,71 @@
     inverse = lax.rsqrt(square * (1.0 / WID) + 1e-06)
     for k in range(0, WID, 512):
         cols = pl.ds(k, 512)
-        nrm[:, cols] = (att[:, cols] * inverse * gain_ref[:, cols]).astype(bf16)
-
-    experts = lax.broadcasted_iota(jnp.int32, (16, 128), 0)
-    route = [routes_ref[pl.ds(k, 1), :] for k in range(2)]
-    hot = [(r == experts).astype(f32) for r in route]
+        value = (att[:, cols] * inverse * gain_ref[:, cols]).astype(bf16)
+        if k < AW:
+            nrm[:, cols] = value
+        else:
+            toks[y, :, pl.ds(k - AW, 512)] = value
+
+    route = [routes_ref[pl.ds(k, 1), :].astype(f32) for k in range(2)]
+    infos[y] = jnp.concatenate(route + [jnp.zeros((6, 128), f32)], axis=0)
+
+    def token_copies(d):
+        return [
+            pltpu.make_async_remote_copy(
+                src_ref=infos.at[y], dst_ref=infos.at[y], send_sem=isend.at[d], recv_sem=irecv.at[d],
+                device_id=(s, lane(d, c)), device_id_type=MESH,
+            ),
+            pltpu.make_async_remote_copy(
+                src_ref=toks.at[y], dst_ref=toks.at[y], send_sem=tsend.at[d], recv_sem=trecv.at[d],
+                device_id=(s, lane(d, c)), device_id_type=MESH,
+            ),
+        ]
+
+    pl.semaphore_wait(barrier, len(others) + 4)
+    for d in (1, 3, 2):
+        for copy in token_copies(d):
+            copy.start()
+
+    experts = lax.broadcasted_iota(jnp.int32, (16, 128), 0).astype(f32)
     row_id = lax.broadcasted_iota(jnp.int32, (128, 128), 0)
     col_id = lax.broadcasted_iota(jnp.int32, (128, 128), 1)
     earlier = (row_id < col_id).astype(f32).astype(bf16)
-    before = jnp.dot((hot[0] + hot[1]).astype(bf16), earlier, preferred_element_type=f32)
     place = lax.broadcasted_iota(jnp.int32, (256, 128), 0).astype(f32)
-    main_hit, rem_hit = [], []
-    for k in range(2):
-        slot = jnp.sum(before * hot[k], axis=0, keepdims=True)
-        base = route[k].astype(f32) * 16.0 + slot
-        low = slot < float(MAIN)
-        main_hit.append((jnp.where(low, base, -1.0) == place).astype(f32))
-        rem_hit.append([
-            (jnp.where(low, -1.0, base + (4.0 * j - 16.0)) == place).astype(f32) for j in range(4)
-        ])
+
+    def hits(routes_of, parts):
+        hot = [(r == experts).astype(f32) for r in routes_of]
+        before = jnp.dot((hot[0] + hot[1]).astype(bf16), earlier, preferred_element_type=f32)
+        main, rem = [], []
+        for k in range(2):
+            slot = jnp.sum(before * hot[k], axis=0, keepdims=True)
+            base = routes_of[k] * 16.0 + slot
+            low = slot < float(MAIN)
+            main.append((jnp.where(low, base, -1.0) == place).astype(f32))
+            rem.append([
+                (jnp.where(low, -1.0, base + (4.0 * j - 16.0)) == place).astype(f32) for j in parts
+            ])
+        return main, rem
+
+    main_hit, rem_hit = hits(route, range(4))
     weight = [rw_ref[pl.ds(k, 1), :] for k in range(2)]
     over_rows = (((0,), (0,)), ((), ()))
     chosen = (main_hit[0] + main_hit[1]).astype(bf16)
-    for k in range(0, WID, 512):
+    for k in range(0, AW, 512):
         cols = pl.ds(k, 512)
         outg[:, cols] = jnp.dot(chosen, nrm[:, cols], preferred_element_type=f32).astype(bf16)
-    extra = jnp.zeros((256, REM), f32)
+    extra = jnp.zeros((256, REMA), f32)
     for j in range(4):
         extra = extra + jnp.dot(
-            (rem_hit[0][j] + rem_hit[1][j]).astype(bf16), nrm[:, pl.ds(j * REM, REM)],
+            (rem_hit[0][j] + rem_hit[1][j]).astype(bf16), nrm[:, pl.ds(j * REMA, REMA)],
             preferred_element_type=f32,
         )
-    outg[:, pl.ds(WID, REM)] = extra.astype(bf16)
+    outg[:, pl.ds(AW, REMA)] = extra.astype(bf16)
 
     def keep_split(ref, value):
         high = value.astype(bf16)
         ref[pl.ds(0, 256), :] = high
         ref[pl.ds(256, 256), :] = (value - high.astype(f32)).astype(bf16)
-
-    pl.semaphore_wait(barrier, len(others) + 3)
 
     def band(device):
         return pl.ds(pl.multiple_of(device * MAIN, MAIN), MAIN)
@@ -551,7 +580,7 @@
         return pl.ds(pl.multiple_of(position * CH, 16), CH)
 
     def x_copy(g, position, part, send, to, slot=None):
-        cols = pl.ds(0, WID) if part == 2 else pl.ds(part * HW, HW)
+        cols = pl.ds(0, AW) if part == 2 else pl.ds(part * AH, AH)
         return pltpu.make_async_remote_copy(
             src_ref=xs.at[g, rows_of(position), cols], dst_ref=xs.at[g, rows_of(position), cols],
             send_sem=xsend.at[g, send], recv_sem=xrecv.at[g, position, part % 2],
@@ -576,11 +605,11 @@
                 plane_copy(outg, arr, psend, precv, s, at(GROUPS[g], dx)).wait_recv()
         rows = group_rows(g)
         first = pl.multiple_of(t * CH, 16)
-        for k in range(0, WID, 512):
+        for k in range(0, AW, 512):
             xs[g, pl.ds(first, 64), pl.ds(k, 512)] = arr[rows, pl.ds(k, 512)]
         for j in range(4):
-            xs[g, pl.ds(first + 64, 16), pl.ds(j * REM, REM)] = jnp.dot(
-                fold[j], arr[rows, pl.ds(WID, REM)], preferred_element_type=f32
+            xs[g, pl.ds(first + 64, 16), pl.ds(j * REMA, REMA)] = jnp.dot(
+                fold[j], arr[rows, pl.ds(AW, REMA)], preferred_element_type=f32
             ).astype(bf16)
         for copy in x_sends(g)[:3]:
             x_copy(*copy).start()
@@ -599,6 +628,70 @@
         x_copy(g, lane(2, c), 1, 0, t).wait_recv()
         x_copy(*x_sends(g)[7]).start()
 
+    def slot_copy(to, sender):
+        return pltpu.make_async_remote_copy(
+            src_ref=outb.at[to], dst_ref=arrb.at[sender],
+            send_sem=obsend.at[to], recv_sem=obrecv.at[sender],
+            device_id=(to, t), device_id_type=MESH,
+        )
+
+    def spread(_):
+        for d in (1, 3, 2):
+            for copy in token_copies(d):
+                copy.wait_recv()
+        mains, rems = [], []
+        for yy in range(4):
+            main, rem = hits([infos[yy, pl.ds(k, 1), :] for k in range(2)], (yy,))
+            mains.append((main[0] + main[1]).astype(bf16))
+            rems.append((rem[0][0] + rem[1][0]).astype(bf16))
+        rems = jnp.concatenate(rems, axis=1)
+        for k in range(0, WID - AW, 512):
+            cols = pl.ds(k, 512)
+            for yy in range(4):
+                value = jnp.dot(mains[yy], toks[yy, :, cols], preferred_element_type=f32)
+                outb[:, pl.ds(16 * yy, 16), cols] = value.astype(bf16).reshape(16, 16, 512)
+            every = jnp.concatenate([toks[yy, :, cols] for yy in range(4)], axis=0)
+            value = jnp.dot(rems, every, preferred_element_type=f32)
+            outb[:, pl.ds(64, 16), cols] = value.astype(bf16).reshape(16, 16, 512)
+        for dz, dx in others:
+            slot_copy(at(-dz, -dx), s).start()
+        arrb[s] = outb[s]
+
+    move_row = lax.broadcasted_iota(jnp.int32, (64, 64), 0)
+    move_col = lax.broadcasted_iota(jnp.int32, (64, 64), 1)
+    move = (
+        move_col == 16 * ((move_row >> 2) & 3) + 4 * (move_row >> 4) + (move_row & 3)
+    ).astype(f32).astype(bf16)
+
+    def far_copy(g, yy, core):
+        cols = pl.ds(AW, WID - AW)
+        return pltpu.make_async_remote_copy(
+            src_ref=xs.at[g, rows_of(2 * yy + core), cols], dst_ref=xs.at[g, rows_of(2 * yy + core), cols],
+            send_sem=xbsend.at[g, yy], recv_sem=xbrecv.at[g, yy],
+            device_id=(s, mate), device_id_type=MESH,
+        )
+
+    def gather(g):
+        for dx in (0, 1, -1, 2):
+            if (GROUPS[g], dx) != (0, 0):
+                slot_copy(s, at(GROUPS[g], dx)).wait_recv()
+        first = ((z + GROUPS[g] + NZ) % NZ) * NX
+        moved = []
+        for k in range(0, WID - AW, 512):
+            cols = pl.ds(k, 512)
+            tails = jnp.concatenate([arrb[first + xx, pl.ds(64, 16), cols] for xx in range(4)], axis=0)
+            moved.append(jnp.dot(move, tails, preferred_element_type=f32).astype(bf16))
+        for yy in range(4):
+            row = pl.multiple_of((2 * yy + c) * CH, 16)
+            for i, k in enumerate(range(0, WID - AW, 512)):
+                into = pl.ds(AW + k, 512)
+                for xx in range(4):
+                    xs[g, pl.ds(row + 16 * xx, 16), into] = arrb[
+                        first + xx, pl.ds(16 * yy, 16), pl.ds(k, 512)
+                    ]
+                xs[g, pl.ds(row + 64, 16), into] = moved[i][16 * yy:16 * yy + 16]
+            far_copy(g, yy, c).start()
+
     def pair_copy(g, yy):
         return pltpu.make_async_remote_copy(
             src_ref=ps.at[g, rows_of(2 * yy + 1 - c), :], dst_ref=pr.at[g, yy],
@@ -611,6 +704,8 @@
     def compute(g):
         for dy in (0, -1, 1, 2):
             x_copy(g, lane(dy, 1 - c), 2, 0, t).wait_recv()
+        for yy in range(4):
+            far_copy(g, yy, 1 - c).wait_recv()
         if g == 0:
             for load in loads[1:]:
                 load.wait()
@@ -702,10 +797,12 @@
                 plane_copy(reto, ret, bsend, brecv, to, s).start()
 
     for stage, g in (
-        (build, 0), (build, 1), (forward, 0), (build, 2), (forward, 1), (build, 3), (far, 0),
-        (compute, 0), (pair, 0), (forward, 2), (far, 1), (compute, 1), (pair, 1), (middle, 0),
-        (forward, 3), (far, 2), (compute, 2), (pair, 2), (finish, 0), (middle, 1), (far, 3),
-        (compute, 3), (pair, 3), (middle, 2), (finish, 1), (middle, 3), (finish, 2), (finish, 3),
+        (build, 0), (build, 1), (spread, 0), (forward, 0), (build, 2), (forward, 1), (build, 3),
+        (far, 0), (gather, 0), (compute, 0), (pair, 0),
+        (forward, 2), (far, 1), (gather, 1), (compute, 1), (pair, 1), (middle, 0),
+        (forward, 3), (far, 2), (gather, 2), (compute, 2), (pair, 2), (finish, 0), (middle, 1),
+        (far, 3), (gather, 3), (compute, 3), (pair, 3), (middle, 2), (finish, 1), (middle, 3),
+        (finish, 2), (finish, 3),
     ):
         stage(g)
 
@@ -725,11 +822,16 @@
     for dz, dx in others:
         plane_copy(outg, arr, psend, precv, at(dz, dx), s).wait_send()
         plane_copy(reto, ret, bsend, brecv, at(dz, dx), s).wait_send()
+        slot_copy(at(dz, dx), s).wait_send()
+    for d in (1, 2, 3):
+        for copy in token_copies(d):
+            copy.wait_send()
     for g in range(4):
         for copy in x_sends(g):
             x_copy(*copy).wait_send()
         for yy in range(4):
             pair_copy(g, yy).wait_send()
+            far_copy(g, yy, c).wait_send()
         for copy in r_sends(g):
             r_copy(*copy).wait_send()
 
@@ -752,14 +854,18 @@
             pltpu.VMEM((1, WID), f32),
             pltpu.VMEM((2, 128), jnp.int32),
             pltpu.VMEM((2, 128), f32),
+            pltpu.VMEM((4, 8, 128), f32),
+            pltpu.VMEM((4, 128, WID - AW), bf16),
+            pltpu.VMEM((16, CH, WID - AW), bf16),
+            pltpu.VMEM((16, CH, WID - AW), bf16),
             pltpu.VMEM((1024, WID), bf16),
             pltpu.VMEM((WID, 640), bf16),
             pltpu.VMEM((WID, 640), bf16),
             pltpu.VMEM((640, WID), bf16),
             pltpu.VMEM((128, WID), f32),
-            pltpu.VMEM((128, WID), bf16),
-            pltpu.VMEM((256, BAND), bf16),
-            pltpu.VMEM((256, BAND), bf16),
+            pltpu.VMEM((128, AW), bf16),
+            pltpu.VMEM((256, AW + REMA), bf16),
+            pltpu.VMEM((256, AW + REMA), bf16),
             pltpu.VMEM((256, BAND), bf16),
             pltpu.VMEM((256, BAND), bf16),
             pltpu.VMEM((4, NT * CH, WID), bf16),
@@ -771,6 +877,8 @@
             pltpu.VMEM((512, 128), bf16),
             pltpu.VMEM((4, 512, 128), bf16),
             dma((9,)),
+            dma((4,)), dma((4,)), dma((4,)), dma((4,)),
+            dma((16,)), dma((16,)), dma((4, 4)), dma((4, 4)),
             dma((16,)), dma((16,)),
             dma((4, 8)), dma((4, 8, 2)),
             dma((4, 4)), dma((4, 4)),

time: 179 us -> 170 us (0.950)
  Pallas kernels: 177 us -> 168 us
    pallas_call x1, Pallas kernels: 115 us -> 106 us  [routed_experts(): pl.pallas_call(expert_kernel, out_shape=jax.ShapeDtypeStruct((128, WID),...]
where the time goes in v5:
time: 170 us
  Pallas kernels  168 us (99%)
  local copies, waits for them, and re-layouts  1.88 us (1%)
    pallas_call x1, Pallas kernels, routed_experts(): pl.pallas_call(expert_kernel, out_shape=jax.ShapeDtypeStruct((128, WID),...  106 us
    pallas_call x1, Pallas kernels, attention(): pl.pallas_call(attention_kernel, out_shape=jax.ShapeDtypeStruct((128, 102...  61.4 us

profile of v5, /device:TPU:1, one launch (start us, length us, event | category | flops | bytes accessed | tf_op | source)
XLA Modules:
  0.0 170.1 jit_solution(8818241196254679753)
XLA Ops:
  0.7 61.4 %attention.1.heads_hbm = bf16[128,1024]{1,0:T(8,128)(2,1)} custom-call(f32[1]{0:T(128)S(6)} %copy.15.lam_hbm, f32[1,128]{1,0:T(1,128)} %bitcast.7, bf16[1024,128]{1,0:T(8,128)(2,1)} %q_hbm.1, bf16[1024,128]{1,0:T(8,128)(2,1)} %k_hbm.1, bf16[1024,128]{1,0:T(8,128)(2,1)} %v_hbm.1), custom_call_target="tpu_custom_call" | custom-call | tf_op jit(solution)/shard_map/attention/pallas_call | solution.py:380
  62.1 106.1 %experts.1 = bf16[128,2048]{1,0:T(8,128)(2,1)} custom-call(bf16[128,1024]{1,0:T(8,128)(2,1)} %attention.1.heads_hbm, bf16[128,2048]{1,0:T(8,128)(2,1)} %stream_hbm.1, f32[1,2048]{1,0:T(1,128)} %bitcast.4, s32[2,128]{1,0:T(2,128)} %bitcast.5, f32[2,128]{1,0:T(2,128)} %bitcast.6, bf16[1024,2048]{1,0:T(8,128)(2,1)} %ow_hbm.1, bf16[1,2048,640]{2,1,0:T(8,128)(2,1)} %gate_hbm.1, ...), custom_call_target="tpu_custom_call" | custom-call | tf_op jit(solution)/shard_map/experts/pallas_call | solution.py:846
  168.2 1.9 %copy.16 = bf16[128,2048]{1,0:T(8,128)(2,1)} copy(bf16[128,2048]{1,0:T(8,128)(2,1)} %experts.1) | data formatting | bytes 1048576

commit v6 on v5

--- a/solution.py
+++ b/solution.py
@@ -19,7 +19,7 @@
 NEG = -1e30
 VROWS = 144
 TQ = 512
-KB = 256
+KB = 512
 WORK = (
     (0, 0), (3, 0), (1, 0), (3, 3), (3, 1), (1, 3), (1, 1), (3, 2), (1, 2),
     (2, 0), (2, 3), (2, 1), (2, 2), (0, 3), (0, 1), (0, 2),
@@ -229,7 +229,7 @@
         some = total > 0.0
         safe = jnp.where(some, total, 1.0)
         level = jnp.where(some, mx[e, d, m] + jnp.log2(safe), NEG)
-        return acc[e, d, m, pl.ds(0, 128), :] / safe, level
+        return acc[e, d, m, pl.ds(0, 128), :] * (1.0 / safe), level
 
     def send_partial(d):
         for e in range(2):
@@ -245,13 +245,18 @@
             for kind in (1, 0, 2):
                 settle(kind, 0)
         if n == 1:
-            for kind in range(3):
+            for kind in (0, 1):
                 for slot in (3, 1):
                     arrive(kind, slot)
-            for kind in range(3):
+            for slot in (3, 1):
+                settle(0, slot)
+        if n == 3:
+            for slot in (3, 1):
+                arrive(2, slot)
+            for kind in (1, 2):
                 for slot in (3, 1):
                     settle(kind, slot)
-        if n == 5:
+        if n == 6:
             for kind in range(3):
                 arrive(kind, 2)
             for kind in range(3):
@@ -264,7 +269,7 @@
             send_partial(2)
 
     def step(n, carry):
-        for k in (0, 1, 5, 8, 9, 13):
+        for k in (0, 1, 3, 6, 8, 9, 13):
             @pl.when(n == k)
             def _(k=k):
                 before(k)
@@ -419,12 +424,12 @@
     )(lambdas, head_gain.reshape(1, -1), queries, key_rows, value_rows)
 
 
-GROUPS = (0, -1, 1, 2)
+GROUPS = (1, 2, -1, 0)
 MAIN = 16
 CH = 80
 WID = 2048
 HW = 1024
-AW = 1024
+AW = 1536
 AH = AW // 2
 REMA = AW // 4
 REM = 512
@@ -435,7 +440,7 @@
 def expert_kernel(
     heads_hbm, stream_hbm, gain_hbm, routes_hbm, rw_hbm, ow_hbm, gate_hbm, up_hbm, down_hbm,
     out_ref,
-    heads_ref, stream_ref, gain_ref, routes_ref, rw_ref, infos, toks, outb, arrb, ow, gw, uw, dw, att, nrm, outg, arr, reto, ret, xs, act, ps, pr, rh, rf, cm, cr,
+    heads_ref, stream_ref, gain_ref, routes_ref, rw_ref, infos, toks, outb, arrb, ow, guw, dw, att, nrm, outg, arr, reto, ret, xs, act, ps, pr, rh, rf, cm, cr,
     load_sem, isend, irecv, tsend, trecv, obsend, obrecv, xbsend, xbrecv, psend, precv, xsend, xrecv, qsend, qrecv, rsend, rhrecv, rfrecv, bsend, brecv,
 ):
     s = lax.axis_index("sp")
@@ -453,8 +458,8 @@
 
     loads = [
         pltpu.make_async_copy(ow_hbm, ow, load_sem.at[0]),
-        pltpu.make_async_copy(gate_hbm.at[0], gw, load_sem.at[1]),
-        pltpu.make_async_copy(up_hbm.at[0], uw, load_sem.at[2]),
+        pltpu.make_async_copy(gate_hbm.at[0], guw.at[:, pl.ds(0, 640)], load_sem.at[1]),
+        pltpu.make_async_copy(up_hbm.at[0], guw.at[:, pl.ds(640, 640)], load_sem.at[2]),
         pltpu.make_async_copy(down_hbm.at[0], dw, load_sem.at[3]),
     ]
     small = [
@@ -715,8 +720,8 @@
             yy = (y + dy) % 4
             rows = pl.ds(pl.multiple_of(yy * 2 * CH, 32), 2 * CH)
             value = xs[g, rows, :]
-            gate = jnp.dot(value, gw[...], preferred_element_type=f32)
-            upper = jnp.dot(value, uw[...], preferred_element_type=f32)
+            both = jnp.dot(value, guw[...], preferred_element_type=f32)
+            gate, upper = both[:, :640], both[:, 640:]
             act[...] = (gate / (1.0 + jnp.exp(-gate)) * upper).astype(bf16)
             ps[g, rows, :] = jnp.dot(act[...], dw[...], preferred_element_type=f32).astype(bf16)
             pair_copy(g, yy).start()
@@ -796,28 +801,38 @@
             else:
                 plane_copy(reto, ret, bsend, brecv, to, s).start()
 
+    def collect(g):
+        for dx in (0, 1, -1, 2):
+            if (GROUPS[g], dx) != (0, 0):
+                plane_copy(reto, ret, bsend, brecv, s, at(-GROUPS[g], dx)).wait_recv()
+        first = ((z - GROUPS[g] + NZ) % NZ) * 64
+        rows = pl.ds(pl.multiple_of(first, 64), 64)
+        low = pl.ds(pl.multiple_of(first + 256, 64), 64)
+        factor = jnp.concatenate([cm[rows, :], cm[low, :]], axis=0)
+        tail = ret[rows, pl.ds(WID, REM)]
+        for j in range(4):
+            cols = pl.ds(j * REM, REM)
+            back = ret[rows, cols]
+            routed = lax.dot_general(
+                jnp.concatenate([factor, cr[j, rows, :], cr[j, low, :]], axis=0),
+                jnp.concatenate([back, back, tail, tail], axis=0), over_rows,
+                preferred_element_type=f32,
+            )
+            if g == 3:
+                out_ref[:, cols] = (att[:, cols] + routed).astype(bf16)
+            else:
+                att[:, cols] = att[:, cols] + routed
+
     for stage, g in (
-        (build, 0), (build, 1), (spread, 0), (forward, 0), (build, 2), (forward, 1), (build, 3),
-        (far, 0), (gather, 0), (compute, 0), (pair, 0),
-        (forward, 2), (far, 1), (gather, 1), (compute, 1), (pair, 1), (middle, 0),
-        (forward, 3), (far, 2), (gather, 2), (compute, 2), (pair, 2), (finish, 0), (middle, 1),
-        (far, 3), (gather, 3), (compute, 3), (pair, 3), (middle, 2), (finish, 1), (middle, 3),
-        (finish, 2), (finish, 3),
+        (build, 0), (build, 1), (spread, 0), (forward, 0), (build, 2), (forward, 1),
+        (build, 3), (far, 0), (gather, 0), (compute, 0), (pair, 0), (forward, 2),
+        (far, 1), (gather, 1), (compute, 1), (pair, 1), (middle, 0), (forward, 3),
+        (far, 2), (gather, 2), (compute, 2), (middle, 1), (pair, 2), (finish, 0),
+        (far, 3), (gather, 3), (compute, 3), (middle, 2), (pair, 3), (finish, 1),
+        (middle, 3), (finish, 2), (finish, 3), (collect, 0), (collect, 1), (collect, 2),
+        (collect, 3),
     ):
         stage(g)
-
-    for dz, dx in others:
-        plane_copy(reto, ret, bsend, brecv, s, at(dz, dx)).wait_recv()
-    for j in range(4):
-        cols = pl.ds(j * REM, REM)
-        back = ret[:, cols]
-        tail = ret[:, pl.ds(WID, REM)]
-        routed = lax.dot_general(
-            cm[...], jnp.concatenate([back, back], axis=0), over_rows, preferred_element_type=f32
-        ) + lax.dot_general(
-            cr[j], jnp.concatenate([tail, tail], axis=0), over_rows, preferred_element_type=f32
-        )
-        out_ref[:, cols] = (att[:, cols] + routed).astype(bf16)
 
     for dz, dx in others:
         plane_copy(outg, arr, psend, precv, at(dz, dx), s).wait_send()
@@ -859,8 +874,7 @@
             pltpu.VMEM((16, CH, WID - AW), bf16),
             pltpu.VMEM((16, CH, WID - AW), bf16),
             pltpu.VMEM((1024, WID), bf16),
-            pltpu.VMEM((WID, 640), bf16),
-            pltpu.VMEM((WID, 640), bf16),
+            pltpu.VMEM((WID, 1280), bf16),
             pltpu.VMEM((640, WID), bf16),
             pltpu.VMEM((128, WID), f32),
             pltpu.VMEM((128, AW), bf16),

time: 170 us -> 167 us (0.982)
  Pallas kernels: 168 us -> 164 us
    pallas_call x1, Pallas kernels: 61.4 us -> 59.6 us  [attention(): pl.pallas_call(attention_kernel, out_shape=jax.ShapeDtypeStruct((128, 102...]
where the time goes in v6:
time: 167 us
  Pallas kernels  164 us (98%)
  local copies, waits for them, and re-layouts  1.88 us (1%)
    pallas_call x1, Pallas kernels, routed_experts(): pl.pallas_call(expert_kernel, out_shape=jax.ShapeDtypeStruct((128, WID),...  105 us
    pallas_call x1, Pallas kernels, attention(): pl.pallas_call(attention_kernel, out_shape=jax.ShapeDtypeStruct((128, 102...  59.6 us

profile of v6, /device:TPU:1, one launch (start us, length us, event | category | flops | bytes accessed | tf_op | source)
XLA Modules:
  0.0 166.8 jit_solution(11109386841781065559)
XLA Ops:
  0.7 59.6 %attention.1.heads_hbm = bf16[128,1024]{1,0:T(8,128)(2,1)} custom-call(f32[1]{0:T(128)S(6)} %copy.15.lam_hbm, f32[1,128]{1,0:T(1,128)} %bitcast.7, bf16[1024,128]{1,0:T(8,128)(2,1)} %q_hbm.1, bf16[1024,128]{1,0:T(8,128)(2,1)} %k_hbm.1, bf16[1024,128]{1,0:T(8,128)(2,1)} %v_hbm.1), custom_call_target="tpu_custom_call" | custom-call | tf_op jit(solution)/shard_map/attention/pallas_call | solution.py:385
  60.2 104.7 %experts.1 = bf16[128,2048]{1,0:T(8,128)(2,1)} custom-call(bf16[128,1024]{1,0:T(8,128)(2,1)} %attention.1.heads_hbm, bf16[128,2048]{1,0:T(8,128)(2,1)} %stream_hbm.1, f32[1,2048]{1,0:T(1,128)} %bitcast.4, s32[2,128]{1,0:T(2,128)} %bitcast.5, f32[2,128]{1,0:T(2,128)} %bitcast.6, bf16[1024,2048]{1,0:T(8,128)(2,1)} %ow_hbm.1, bf16[1,2048,640]{2,1,0:T(8,128)(2,1)} %gate_hbm.1, ...), custom_call_target="tpu_custom_call" | custom-call | tf_op jit(solution)/shard_map/experts/pallas_call | solution.py:861
  164.9 1.9 %copy.16 = bf16[128,2048]{1,0:T(8,128)(2,1)} copy(bf16[128,2048]{1,0:T(8,128)(2,1)} %experts.1) | data formatting | bytes 1048576

commit v7 on v6

--- a/solution.py
+++ b/solution.py
@@ -424,7 +424,7 @@
     )(lambdas, head_gain.reshape(1, -1), queries, key_rows, value_rows)
 
 
-GROUPS = (1, 2, -1, 0)
+GROUPS = (0, 1, 2, -1)
 MAIN = 16
 CH = 80
 WID = 2048

time: 167 us -> 163 us (0.976)
  Pallas kernels: 164 us -> 160 us
    pallas_call x1, Pallas kernels: 105 us -> 101 us  [routed_experts(): pl.pallas_call(expert_kernel, out_shape=jax.ShapeDtypeStruct((128, WID),...]
where the time goes in v7:
time: 163 us
  Pallas kernels  160 us (98%)
  local copies, waits for them, and re-layouts  1.88 us (1%)
    pallas_call x1, Pallas kernels, routed_experts(): pl.pallas_call(expert_kernel, out_shape=jax.ShapeDtypeStruct((128, WID),...  101 us
    pallas_call x1, Pallas kernels, attention(): pl.pallas_call(attention_kernel, out_shape=jax.ShapeDtypeStruct((128, 102...  59.6 us

profile of v7, /device:TPU:1, one launch (start us, length us, event | category | flops | bytes accessed | tf_op | source)
XLA Modules:
  0.0 162.8 jit_solution(9811686910631762748)
XLA Ops:
  0.7 59.6 %attention.1.heads_hbm = bf16[128,1024]{1,0:T(8,128)(2,1)} custom-call(f32[1]{0:T(128)S(6)} %copy.15.lam_hbm, f32[1,128]{1,0:T(1,128)} %bitcast.7, bf16[1024,128]{1,0:T(8,128)(2,1)} %q_hbm.1, bf16[1024,128]{1,0:T(8,128)(2,1)} %k_hbm.1, bf16[1024,128]{1,0:T(8,128)(2,1)} %v_hbm.1), custom_call_target="tpu_custom_call" | custom-call | tf_op jit(solution)/shard_map/attention/pallas_call | solution.py:385
  60.2 100.7 %experts.1 = bf16[128,2048]{1,0:T(8,128)(2,1)} custom-call(bf16[128,1024]{1,0:T(8,128)(2,1)} %attention.1.heads_hbm, bf16[128,2048]{1,0:T(8,128)(2,1)} %stream_hbm.1, f32[1,2048]{1,0:T(1,128)} %bitcast.4, s32[2,128]{1,0:T(2,128)} %bitcast.5, f32[2,128]{1,0:T(2,128)} %bitcast.6, bf16[1024,2048]{1,0:T(8,128)(2,1)} %ow_hbm.1, bf16[1,2048,640]{2,1,0:T(8,128)(2,1)} %gate_hbm.1, ...), custom_call_target="tpu_custom_call" | custom-call | tf_op jit(solution)/shard_map/experts/pallas_call | solution.py:861
  160.9 1.9 %copy.16 = bf16[128,2048]{1,0:T(8,128)(2,1)} copy(bf16[128,2048]{1,0:T(8,128)(2,1)} %experts.1) | data formatting | bytes 1048576
